TPU v7x, 32 devices: a whole 2x2x4 slice. The times are simulated.
32 devices in a mesh: rep: 2 (over x), fs: 8 (over z, y), tp: 2 (over core).
Axes of the slice: x: 2, y: 2, z: 4, core: 2. Of those that a mesh axis runs over, the one named last changes fastest.
Arguments:
- tokens: bfloat16 [8192, 2048], P(('rep', 'fs')), may hold values from -6 to 6
- mix_gain: float32 [2048], replicated, may hold values from 0.1 to 1.9
- gate_proj: bfloat16 [2048, 1024], P('fs', 'tp'), may hold values from -0.125 to 0.125
- value_proj: bfloat16 [2048, 1024], P('fs', 'tp'), may hold values from -0.125 to 0.125
- value_gain: float32 [1024], P('tp'), may hold values from 0.1 to 1.9
- value_shift: float32 [1024], P('tp'), may hold values from -3 to 3
- spatial_weight: bfloat16 [4, 128, 128], replicated, may hold values from -0.5 to 0.5
- spatial_shift: float32 [4, 128], replicated, may hold values from 0.1 to 1.9
- out_proj: bfloat16 [1024, 2048], P('tp', 'fs'), may hold values from -0.1875 to 0.1875
- ffn_gain: float32 [2048], replicated, may hold values from 0.1 to 1.9
- up_proj: bfloat16 [2048, 8192], P('fs', 'tp'), may hold values from -0.125 to 0.125
- down_proj: bfloat16 [8192, 2048], P('tp', 'fs'), may hold values from -0.0625 to 0.0625
Outputs:
- layer_out: bfloat16 [8192, 2048], P(('rep', 'fs'))
All inputs are finite; a program needn't handle non-finite values.
Results may differ from a plain program's by a relative error of at most 0.018.
Values may be sent and summed in bfloat16 or wider, within the bound.
A program may use at most 128 MiB of HBM per device.

v0:
```python
import jax
import jax.numpy as jnp
from jax import lax
from jax.sharding import PartitionSpec as P


GW = 1024
GROUPS = 4
BLOCK = 128
SIDE = 2


EPS = 1e-06


def rms_norm(values, scale):
    floats = values.astype(jnp.float32)
    return (
        floats * lax.rsqrt(jnp.mean(floats * floats, axis=-1, keepdims=True) + EPS) * scale
    ).astype(jnp.bfloat16)


def body(
    tokens,
    mix_gain,
    gate_proj,
    value_proj,
    value_gain,
    value_shift,
    spatial_weight,
    spatial_shift,
    out_proj,
    ffn_gain,
    up_proj,
    down_proj,
):
    normed = rms_norm(tokens, mix_gain)
    rows = normed.shape[0]
    cols = gate_proj.shape[1]
    pieces = (
        lax.all_gather(gate_proj, "fs", axis=0, tiled=True),
        lax.all_gather(value_proj, "fs", axis=0, tiled=True),
    )
    columns = normed
    gate_acc = jnp.dot(columns, pieces[0], preferred_element_type=jnp.float32)
    value_acc = jnp.dot(columns, pieces[1], preferred_element_type=jnp.float32)
    gate = jax.nn.gelu(gate_acc)
    value = jax.nn.gelu(value_acc)
    sums, squares = lax.psum((jnp.sum(value, axis=-1), jnp.sum(value * value, axis=-1)), "tp")
    centre = (sums / GW)[:, None]
    spread = (squares / GW)[:, None] - centre * centre
    leveled = ((value - centre) * lax.rsqrt(spread + EPS) * value_gain + value_shift).astype(
        jnp.bfloat16
    )
    group_width = GW // GROUPS
    span = min(cols, group_width)
    count = cols // span
    first = lax.axis_index("tp") * cols // group_width
    lower = jnp.tril(lax.dynamic_slice_in_dim(spatial_weight, first, count, 0))
    offsets = lax.dynamic_slice_in_dim(spatial_shift, first, count, 0)
    pieces = leveled.reshape(rows // BLOCK, BLOCK, count, span)
    mixed = (
        jnp.einsum("gts,nsgw->ntgw", lower, pieces, preferred_element_type=jnp.float32)
        + offsets.T[None, :, :, None]
    )
    gated = (gate * mixed.reshape(rows, cols)).astype(jnp.bfloat16)
    out_whole = lax.all_gather(out_proj, "fs", axis=1, tiled=True)
    mixer_terms = jnp.dot(gated, out_whole, preferred_element_type=jnp.float32)
    mixer_total = lax.psum(mixer_terms.astype(jnp.bfloat16), "tp").astype(jnp.float32)
    midway = (tokens.astype(jnp.float32) + mixer_total).astype(jnp.bfloat16)
    normed2 = rms_norm(midway, ffn_gain)
    columns = normed2
    hidden_acc = jnp.dot(
        columns,
        lax.all_gather(up_proj, "fs", axis=0, tiled=True),
        preferred_element_type=jnp.float32,
    )
    hidden = jnp.square(jax.nn.relu(hidden_acc)).astype(jnp.bfloat16)
    down_whole = lax.all_gather(down_proj, "fs", axis=1, tiled=True)
    ffn_terms = jnp.dot(hidden, down_whole, preferred_element_type=jnp.float32)
    ffn_total = lax.psum(ffn_terms.astype(jnp.bfloat16), "tp").astype(jnp.float32)
    return (midway.astype(jnp.float32) + ffn_total).astype(jnp.bfloat16)


def fast_body(shape, args):
    (
        tokens,
        mix_gain,
        gate_proj,
        value_proj,
        value_gain,
        value_shift,
        spatial_weight,
        spatial_shift,
        out_proj,
        ffn_gain,
        up_proj,
        down_proj,
    ) = args
    f32, bf16 = jnp.float32, jnp.bfloat16
    reps, shards, cores = shape["rep"], shape["fs"], shape["tp"]
    depth = shards // SIDE
    rep, fs, core = lax.axis_index("rep"), lax.axis_index("fs"), lax.axis_index("tp")
    layer, side = fs // SIDE, fs % SIDE
    members = reps * SIDE

    def over_x(a):
        return lax.ppermute(a, "rep", [(i, reps - 1 - i) for i in range(reps)])

    def over_y(a):
        return lax.ppermute(a, "fs", [(i, i ^ 1) for i in range(shards)])

    def over_xy(a):
        pairs = [
            (i * shards + j, (reps - 1 - i) * shards + (j ^ 1))
            for i in range(reps)
            for j in range(shards)
        ]
        return lax.ppermute(a, ("rep", "fs"), pairs)

    def over_z(a, k, layers=None):
        pairs = [(i, i ^ (k * SIDE)) for i in range(shards)]
        return lax.ppermute(
            a, "fs", [p for p in pairs if layers is None or p[0] // SIDE in layers]
        )

    middle = (1, depth - 2)

    inner = (layer == middle[0]) | (layer == middle[1])

    def over_z3(a):
        return over_z(a, 3, middle)

    def relay(second):
        return over_z(second, 1, middle)

    def over_core(a):
        return lax.ppermute(a, "tp", [(i, cores - 1 - i) for i in range(cores)])

    def after(a, *others):
        return lax.optimization_barrier((a,) + others)[0]

    def in_order(mine, other, axis):
        first = jnp.where(side == 0, mine, other)
        second = jnp.where(side == 0, other, mine)
        return jnp.concatenate([first, second], axis)

    def dot(a, b):
        return jnp.dot(a, b, preferred_element_type=f32)

    half_rows = out_proj.shape[0] // reps
    in_width = gate_proj.shape[1]
    carried = jnp.where(rep == 0, gate_proj, value_proj)
    out_half = lax.dynamic_slice_in_dim(out_proj, rep * half_rows, half_rows, 0)
    packed = jnp.concatenate([carried, out_half], 1)
    width = SIDE * gate_proj.shape[0]
    mix_blocks = [packed] + [over_z(packed, k) for k in range(1, depth)]

    slab = up_proj.shape[1] // members

    def up_slab(r, s):
        return lax.dynamic_slice_in_dim(up_proj, (r * SIDE + s) * slab, slab, 1)

    def down_slab(r, s):
        return lax.dynamic_slice_in_dim(down_proj, (r * SIDE + s) * slab, slab, 0)

    up_other = over_y(up_slab(rep, 1 - side))
    up_block = in_order(up_slab(rep, side), up_other, 0)
    up_second = over_z(up_block, 2)
    up_first = over_z(up_block, 1)
    up_third = over_z3(up_block)

    rows = tokens.shape[0] // cores

    def ring_order(a):
        starts = [(layer ^ k) * width for k in range(depth)]
        return jnp.concatenate(
            [lax.dynamic_slice_in_dim(a, s, width, a.ndim - 1) for s in starts], a.ndim - 1
        )

    own = ring_order(lax.dynamic_slice_in_dim(tokens, core * rows, rows, 0))
    normed = rms_norm(own, ring_order(mix_gain))
    mine_acc, other_acc = [0.0, 0.0], [0.0, 0.0]
    outs = []
    for k in range(depth):
        mine = mix_blocks[k] if k == 0 else after(mix_blocks[k], up_other)
        across_x = over_x(mine)
        across_y = over_y(mine)
        across_xy = over_y(across_x) if k == 2 else over_x(across_y)
        pairs = ((mine, across_y), (across_x, across_xy))
        block = jnp.concatenate(
            [in_order(m[:, :in_width], o[:, :in_width], 0) for m, o in pairs]
            + [in_order(m[:, in_width:], o[:, in_width:], 1) for m, o in pairs],
            0,
        )
        columns = normed[:, k * width : (k + 1) * width]
        halves = (block, over_core(block))
        for h in range(cores):
            mine_acc[h] = mine_acc[h] + dot(columns, halves[h][:width])
            other_acc[h] = other_acc[h] + dot(columns, halves[h][width : 2 * width])
        outs.append([m[2 * width :] for m in halves])
    down_other = over_y(after(down_slab(rep, 1 - side), across_x, across_y))
    down_block = in_order(down_slab(rep, side), down_other, 1)
    mine_acc, other_acc = jnp.concatenate(mine_acc, 1), jnp.concatenate(other_acc, 1)
    gate = jax.nn.gelu(jnp.where(rep == 0, mine_acc, other_acc))
    value = jax.nn.gelu(jnp.where(rep == 0, other_acc, mine_acc))
    centre = jnp.mean(value, axis=-1, keepdims=True)
    spread = jnp.mean(value * value, axis=-1, keepdims=True) - centre * centre
    gain = jnp.concatenate([value_gain, over_core(value_gain)])
    shift = jnp.concatenate([value_shift, over_core(value_shift)])
    leveled = ((value - centre) * lax.rsqrt(spread + EPS) * gain + shift).astype(bf16)

    blocks = rows // BLOCK
    row_at = lax.broadcasted_iota(jnp.int32, (rows, rows), 0)
    col_at = lax.broadcasted_iota(jnp.int32, (rows, rows), 1)
    keep = (row_at >= col_at) & (row_at // BLOCK == col_at // BLOCK)
    span = GW // GROUPS
    per_core = GROUPS // cores
    gated = []
    for h in range(cores):
        owner = core if h == 0 else cores - 1 - core
        parts = []
        for i in range(per_core):
            at = owner * per_core + i
            lo = (h * per_core + i) * span
            matrix = lax.dynamic_index_in_dim(spatial_weight, at, 0, False)
            matrix = jnp.where(keep, jnp.tile(matrix, (blocks, blocks)), 0)
            offset = jnp.tile(lax.dynamic_index_in_dim(spatial_shift, at, 0, False), blocks)
            mixed = dot(matrix.astype(bf16), leveled[:, lo : lo + span]) + offset[:, None]
            parts.append((gate[:, lo : lo + span] * mixed).astype(bf16))
        gated.append(
            jnp.concatenate(
                [jnp.where(rep == 0, parts[0], parts[1]), jnp.where(rep == 0, parts[1], parts[0])],
                1,
            )
        )
    mixer = []
    for k in range(depth):
        total = 0.0
        for h in range(cores):
            total = total + dot(gated[h], outs[k][h])
        mixer.append(total)
    midway = (own.astype(f32) + jnp.concatenate(mixer, 1)).astype(bf16)
    normed2 = rms_norm(midway, ring_order(ffn_gain))

    up_relayed = relay(after(up_second, normed2))
    down_ready = after(down_block, normed2)
    down_second = over_z(down_ready, 2)
    down_third = over_z3(down_ready)
    down_first = over_z(down_ready, 1)
    up_blocks = [up_block, up_first, up_second, jnp.where(inner, up_third, up_relayed)]

    cut = rows // 2
    top, bottom = normed2[:cut], normed2[cut:]
    top_x, bottom_y = over_x(top), over_y(bottom)
    top_y, bottom_x = over_y(top), over_x(bottom)
    top_xy, bottom_xy = over_y(top_x), over_x(bottom_y)
    plane = jnp.concatenate(
        [normed2, top_x, bottom_x, top_y, bottom_y, top_xy, bottom_xy], 0
    )
    hidden = []
    for move in (lambda u: u, over_core):
        up_columns = jnp.concatenate([move(u) for u in up_blocks], 0)
        hidden.append(jnp.square(jax.nn.relu(dot(plane, up_columns))).astype(bf16))
    out = jnp.zeros(tokens.shape, bf16)
    part = total = None
    for k in (0, 2, 1, 3):
        if k == 0:
            mine = down_block
        elif k == 2:
            down_relayed = relay(after(down_second, part))
            mine = after(down_second, total)
        elif k == 1:
            mine = after(down_first, total)
        else:
            mine = jnp.where(inner, down_third, after(down_relayed, total))
        part = (dot(hidden[0], mine) + dot(hidden[1], over_core(mine))).astype(bf16)
        total = part[:rows].astype(f32)
        for n, send in enumerate((over_x, over_y, over_xy)):
            total = total + send(part[(n + 1) * rows : (n + 2) * rows]).astype(f32)
        final = (midway[:, k * width : (k + 1) * width].astype(f32) + total).astype(bf16)
        sibling = over_core(final)
        both = jnp.concatenate(
            [jnp.where(core == 0, final, sibling), jnp.where(core == 0, sibling, final)], 0
        )
        out = lax.dynamic_update_slice_in_dim(out, both, (layer ^ k) * width, 1)
    return out


def solution(mesh):
    shape = dict(mesh.shape)

    def step(*args):
        rows = args[0].shape[0]
        fits = shape["rep"] == 2 and shape["tp"] == 2 and shape["fs"] == 4 * SIDE
        if fits and rows % (shape["tp"] * BLOCK) == 0:
            return fast_body(shape, args)
        return body(*args)

    return jax.shard_map(
        step,
        mesh=mesh,
        in_specs=(
            P(("rep", "fs"), None),
            P(),
            P("fs", "tp"),
            P("fs", "tp"),
            P("tp"),
            P("tp"),
            P(),
            P(),
            P("tp", "fs"),
            P(),
            P("fs", "tp"),
            P("tp", "fs"),
        ),
        out_specs=P(("rep", "fs"), None),
        check_vma=False,
    )
```

profile of v0, /device:TPU:0, one launch (start us, length us, event | category | flops | bytes accessed | tf_op | source)
XLA Modules:
  0.0 299.0 jit_solution(41621789571585620)
XLA Ops:
  2.7 3.1 %collective-permute-start.1 = (bf16[256,768]{1,0:T(8,128)(2,1)}, bf16[256,768]{1,0:T(8,128)(2,1)S(1)}, u32[]{:S(2)}, u32[]{:S(2)}) collective-permute-start(bf16[256,768]{1,0:T(8,128)(2,1)} %pad_maximum_fusion.5), channel_id=1, source_target_pairs={{0,4},{2,6},{4,0},{6,2},{8,12},{10,14},{12,8},{14,10},{1,5},{3,7},... | collective-permute-start | bytes 1179656 | tf_op jit(solution)/shard_map/ppermute | solution.py:123
  5.8 1.5 collective-permute-start
  7.3 1.5 collective-permute-start.8
  8.8 2.6 collective-permute-start.4
  11.4 2.0 fusion.177
  14.9 1.9 constant_dynamic-slice_fusion.5
  16.8 1.9 constant_dynamic-slice_fusion
  25.4 1.0 broadcast_select_fusion.46
  26.5 1.0 constant_dynamic-update-slice_fusion.2
  27.9 10.2 %collective-permute-done.2 = bf16[256,1024]{1,0:T(8,128)(2,1)S(1)} collective-permute-done((bf16[256,1024]{1,0:T(8,128)(2,1)}, bf16[256,1024]{1,0:T(8,128)(2,1)S(1)}, u32[]{:S(2)}, u32[]{:S(2)}) %collective-permute-start.2) | collective-permute-done | bytes 524320 | tf_op jit(solution)/shard_map/ppermute | solution.py:111
  39.1 1.5 collective-permute-start.7
  41.1 1.6 collective-permute-start.17
  43.6 14.9 %collective-permute-done.7 = bf16[256,768]{1,0:T(8,128)(2,1)S(1)} collective-permute-done((bf16[256,768]{1,0:T(8,128)(2,1)S(1)}, bf16[256,768]{1,0:T(8,128)(2,1)S(1)}, u32[]{:S(2)}, u32[]{:S(2)}) %collective-permute-start.7) | collective-permute-done | bytes 393248 | tf_op jit(solution)/shard_map/ppermute | solution.py:111
  59.0 1.6 collective-permute-start.29
  61.4 3.8 %collective-permute-done.5 = bf16[256,768]{1,0:T(8,128)(2,1)S(1)} collective-permute-done((bf16[256,768]{1,0:T(8,128)(2,1)S(1)}, bf16[256,768]{1,0:T(8,128)(2,1)S(1)}, u32[]{:S(2)}, u32[]{:S(2)}) %collective-permute-start.5) | collective-permute-done | bytes 393248 | tf_op jit(solution)/shard_map/ppermute | solution.py:111
  66.8 1.6 collective-permute-start.18
  68.9 8.8 %collective-permute-done.12 = bf16[256,768]{1,0:T(8,128)(2,1)S(1)} collective-permute-done((bf16[256,768]{1,0:T(8,128)(2,1)S(1)}, bf16[256,768]{1,0:T(8,128)(2,1)S(1)}, u32[]{:S(2)}, u32[]{:S(2)}) %collective-permute-start.12) | collective-permute-done | bytes 393248 | tf_op jit(solution)/shard_map/ppermute | solution.py:108
  78.8 4.8 %collective-permute-done.18 = bf16[256,768]{1,0:T(8,128)(2,1)S(1)} collective-permute-done((bf16[256,768]{1,0:T(8,128)(2,1)S(1)}, bf16[256,768]{1,0:T(8,128)(2,1)S(1)}, u32[]{:S(2)}, u32[]{:S(2)}) %collective-permute-start.18) | collective-permute-done | bytes 393248 | tf_op jit(solution)/shard_map/ppermute | solution.py:108
  96.2 1.6 collective-permute-start.22
  97.8 4.5 %collective-permute-done.32 = bf16[1024,256]{1,0:T(8,128)(2,1)S(1)} collective-permute-done((bf16[1024,256]{1,0:T(8,128)(2,1)S(1)}, bf16[1024,256]{1,0:T(8,128)(2,1)S(1)}, u32[]{:S(2)}, u32[]{:S(2)}) %collective-permute-start.32) | collective-permute-done | bytes 524320 | tf_op jit(solution)/shard_map/ppermute | solution.py:111
  102.3 1.2 broadcast_select_fusion.3
  103.5 1.6 collective-permute-start.23
  105.2 21.2 %collective-permute-done.28 = bf16[512,1024]{1,0:T(8,128)(2,1)S(1)} collective-permute-done((bf16[512,1024]{1,0:T(8,128)(2,1)S(1)}, bf16[512,1024]{1,0:T(8,128)(2,1)S(1)}, u32[]{:S(2)}, u32[]{:S(2)}) %collective-permute-start.28) | collective-permute-done | bytes 1048608 | tf_op jit(solution)/shard_map/ppermute | solution.py:123
  126.4 1.3 collective-permute-start.24
  128.6 1.5 collective-permute-start.31
  130.2 1.3 collective-permute-start.26
  131.5 9.8 %collective-permute-done.24 = bf16[128,2048]{1,0:T(8,128)(2,1)S(1)} collective-permute-done((bf16[128,2048]{1,0:T(8,128)(2,1)S(1)}, bf16[128,2048]{1,0:T(8,128)(2,1)S(1)}, u32[]{:S(2)}, u32[]{:S(2)}) %collective-permute-start.24) | collective-permute-done | bytes 524320 | tf_op jit(solution)/shard_map/ppermute | solution.py:111
  141.3 11.2 %collective-permute-done.25 = bf16[128,2048]{1,0:T(8,128)(2,1)S(1)} collective-permute-done((bf16[128,2048]{1,0:T(8,128)(2,1)S(1)}, bf16[128,2048]{1,0:T(8,128)(2,1)S(1)}, u32[]{:S(2)}, u32[]{:S(2)}) %collective-permute-start.25) | collective-permute-done | bytes 524320 | tf_op jit(solution)/shard_map/ppermute | solution.py:111
  152.5 1.5 collective-permute-start.27
  154.1 8.8 %collective-permute-done.26 = bf16[128,2048]{1,0:T(8,128)(2,1)S(1)} collective-permute-done((bf16[128,2048]{1,0:T(8,128)(2,1)S(1)}, bf16[128,2048]{1,0:T(8,128)(2,1)S(1)}, u32[]{:S(2)}, u32[]{:S(2)}) %collective-permute-start.26) | collective-permute-done | bytes 524320 | tf_op jit(solution)/shard_map/ppermute | solution.py:111
  162.9 1.8 collective-permute-done.27
  165.8 4.7 %multiply_convert_fusion.1 = bf16[1024,1024]{1,0:T(8,128)(2,1)S(1)} fusion(bf16[1024,2048]{1,0:T(8,128)(2,1)S(1)} %constant_dynamic-update-slice_fusion.16, bf16[2048,1024]{1,0:T(8,128)(2,1)S(1)} %get-tuple-element.33), kind=kOutput, calls=%fused_computation.9 | convolution fusion | flops 4298113024 | bytes 10485760 | tf_op jit(solution)/shard_map/dot_general | solution.py:149
  171.1 4.7 %multiply_convert_fusion = bf16[1024,1024]{1,0:T(8,128)(2,1)S(1)} fusion(bf16[1024,2048]{1,0:T(8,128)(2,1)S(1)} %constant_dynamic-update-slice_fusion.16, bf16[512,1024]{1,0:T(8,128)(2,1)S(1)} %collective-permute-done.36, bf16[512,1024]{1,0:T(8,128)(2,1)S(1)} %collective-permute-done.35, bf16[512,1024]{1,0:T(8,128)(2,1)S(1)} %collective-permute-done.34, ...), kind=kOutput, calls=%fused_computation.8 | convolution fusion | flops 4314890240 | bytes 10485760 | tf_op jit(solution)/shard_map/dot_general | solution.py:149
  175.8 1.2 fusion.185
  177.1 1.2 add_convert_fusion.3
  178.4 1.6 collective-permute-start.38
  180.5 1.5 collective-permute-start.40
  181.9 5.7 %collective-permute-done.38 = bf16[256,512]{1,0:T(8,128)(2,1)S(1)} collective-permute-done((bf16[256,512]{1,0:T(8,128)(2,1)S(1)}, bf16[256,512]{1,0:T(8,128)(2,1)S(1)}, u32[]{:S(2)}, u32[]{:S(2)}) %collective-permute-start.38) | collective-permute-done | bytes 262176 | tf_op jit(solution)/shard_map/ppermute | solution.py:108
  187.6 6.1 %collective-permute-done.39 = bf16[256,512]{1,0:T(8,128)(2,1)S(1)} collective-permute-done((bf16[256,512]{1,0:T(8,128)(2,1)S(1)}, bf16[256,512]{1,0:T(8,128)(2,1)S(1)}, u32[]{:S(2)}, u32[]{:S(2)}) %collective-permute-start.39) | collective-permute-done | bytes 262176 | tf_op jit(solution)/shard_map/ppermute | solution.py:111
  193.9 25.4 %collective-permute-done.42 = bf16[1024,512]{1,0:T(8,128)(2,1)S(1)} collective-permute-done((bf16[1024,512]{1,0:T(8,128)(2,1)S(1)}, bf16[1024,512]{1,0:T(8,128)(2,1)S(1)}, u32[]{:S(2)}, u32[]{:S(2)}) %collective-permute-start.42) | collective-permute-done | bytes 1048608 | tf_op jit(solution)/shard_map/ppermute | solution.py:123
  219.4 2.6 collective-permute-done.43
  221.9 1.2 fusion.186
  223.2 1.2 add_convert_fusion.2
  224.5 1.6 collective-permute-start.44
  226.6 1.5 collective-permute-start.46
  228.1 5.7 %collective-permute-done.44 = bf16[256,512]{1,0:T(8,128)(2,1)S(1)} collective-permute-done((bf16[256,512]{1,0:T(8,128)(2,1)S(1)}, bf16[256,512]{1,0:T(8,128)(2,1)S(1)}, u32[]{:S(2)}, u32[]{:S(2)}) %collective-permute-start.44) | collective-permute-done | bytes 262176 | tf_op jit(solution)/shard_map/ppermute | solution.py:108
  233.7 6.0 %collective-permute-done.45 = bf16[256,512]{1,0:T(8,128)(2,1)S(1)} collective-permute-done((bf16[256,512]{1,0:T(8,128)(2,1)S(1)}, bf16[256,512]{1,0:T(8,128)(2,1)S(1)}, u32[]{:S(2)}, u32[]{:S(2)}) %collective-permute-start.45) | collective-permute-done | bytes 262176 | tf_op jit(solution)/shard_map/ppermute | solution.py:111
  239.9 4.9 %collective-permute-done.48 = bf16[1024,512]{1,0:T(8,128)(2,1)S(1)} collective-permute-done((bf16[1024,512]{1,0:T(8,128)(2,1)S(1)}, bf16[1024,512]{1,0:T(8,128)(2,1)S(1)}, u32[]{:S(2)}, u32[]{:S(2)}) %collective-permute-start.48) | collective-permute-done | bytes 1048608 | tf_op jit(solution)/shard_map/ppermute | solution.py:123
  245.6 1.6 collective-permute-start.55
  247.5 1.2 fusion.187
  248.8 1.2 add_convert_fusion.1
  250.1 1.6 collective-permute-start.50
  252.2 1.5 collective-permute-start.52
  253.6 5.7 %collective-permute-done.50 = bf16[256,512]{1,0:T(8,128)(2,1)S(1)} collective-permute-done((bf16[256,512]{1,0:T(8,128)(2,1)S(1)}, bf16[256,512]{1,0:T(8,128)(2,1)S(1)}, u32[]{:S(2)}, u32[]{:S(2)}) %collective-permute-start.50) | collective-permute-done | bytes 262176 | tf_op jit(solution)/shard_map/ppermute | solution.py:108
  259.3 6.0 %collective-permute-done.51 = bf16[256,512]{1,0:T(8,128)(2,1)S(1)} collective-permute-done((bf16[256,512]{1,0:T(8,128)(2,1)S(1)}, bf16[256,512]{1,0:T(8,128)(2,1)S(1)}, u32[]{:S(2)}, u32[]{:S(2)}) %collective-permute-start.51) | collective-permute-done | bytes 262176 | tf_op jit(solution)/shard_map/ppermute | solution.py:111
  265.6 7.5 %collective-permute-done.55 = bf16[1024,512]{1,0:T(8,128)(2,1)S(1)} collective-permute-done((bf16[1024,512]{1,0:T(8,128)(2,1)S(1)}, bf16[1024,512]{1,0:T(8,128)(2,1)S(1)}, u32[]{:S(2)}, u32[]{:S(2)}) %collective-permute-start.55) | collective-permute-done | bytes 1048608 | tf_op jit(solution)/shard_map/ppermute | solution.py:123
  273.7 2.5 collective-permute-done.41
  276.9 2.6 fusion.188
  279.4 1.3 add_convert_fusion
  280.8 1.6 collective-permute-start.57
  282.8 1.5 collective-permute-start.59
  284.5 5.5 %collective-permute-done.57 = bf16[256,512]{1,0:T(8,128)(2,1)S(1)} collective-permute-done((bf16[256,512]{1,0:T(8,128)(2,1)S(1)}, bf16[256,512]{1,0:T(8,128)(2,1)S(1)}, u32[]{:S(2)}, u32[]{:S(2)}) %collective-permute-start.57) | collective-permute-done | bytes 262176 | tf_op jit(solution)/shard_map/ppermute | solution.py:108
  290.0 6.3 %collective-permute-done.58 = bf16[256,512]{1,0:T(8,128)(2,1)S(1)} collective-permute-done((bf16[256,512]{1,0:T(8,128)(2,1)S(1)}, bf16[256,512]{1,0:T(8,128)(2,1)S(1)}, u32[]{:S(2)}, u32[]{:S(2)}) %collective-permute-start.58) | collective-permute-done | bytes 262176 | tf_op jit(solution)/shard_map/ppermute | solution.py:111
  296.7 1.4 collective-permute-done.60
  (235 shorter events, 39.8 us)
Async XLA Ops:
  2.7 24.8 %collective-permute-start.1 = (bf16[256,768]{1,0:T(8,128)(2,1)}, bf16[256,768]{1,0:T(8,128)(2,1)S(1)}, u32[]{:S(2)}, u32[]{:S(2)}) collective-permute-start(bf16[256,768]{1,0:T(8,128)(2,1)} %pad_maximum_fusion.5), channel_id=1, source_target_pairs={{0,4},{2,6},{4,0},{6,2},{8,12},{10,14},{12,8},{14,10},{1,5},{3,7},... | collective-permute-start | bytes 1179656 | tf_op jit(solution)/shard_map/ppermute | solution.py:123
  5.8 18.1 %collective-permute-start = (bf16[256,768]{1,0:T(8,128)(2,1)}, bf16[256,768]{1,0:T(8,128)(2,1)}, u32[]{:S(2)}, u32[]{:S(2)}) collective-permute-start(bf16[256,768]{1,0:T(8,128)(2,1)} %pad_maximum_fusion.5), channel_id=1, source_target_pairs={{0,2},{2,0},{4,6},{6,4},{8,10},{10,8},{12,14},{14,12},{1,3},{3,1},... | collective-permute-start | bytes 1179656 | tf_op jit(solution)/shard_map/ppermute | solution.py:111
  7.3 33.8 %collective-permute-start.8 = (bf16[256,768]{1,0:T(8,128)(2,1)}, bf16[256,768]{1,0:T(8,128)(2,1)S(1)}, u32[]{:S(2)}, u32[]{:S(2)}) collective-permute-start(bf16[256,768]{1,0:T(8,128)(2,1)} %pad_maximum_fusion.5), channel_id=1, source_target_pairs={{0,16},{16,0},{1,17},{17,1},{2,18},{18,2},{3,19},{19,3},{4,20},{20... | collective-permute-start | bytes 1179656 | tf_op jit(solution)/shard_map/ppermute | solution.py:108
  8.8 30.0 %collective-permute-start.4 = (bf16[256,768]{1,0:T(8,128)(2,1)}, bf16[256,768]{1,0:T(8,128)(2,1)S(1)}, u32[]{:S(2)}, u32[]{:S(2)}) collective-permute-start(bf16[256,768]{1,0:T(8,128)(2,1)} %pad_maximum_fusion.5), channel_id=1, source_target_pairs={{0,8},{2,10},{4,12},{6,14},{8,0},{10,2},{12,4},{14,6},{1,9},{3,11}... | collective-permute-start | bytes 1179656 | tf_op jit(solution)/shard_map/ppermute | solution.py:123
  11.4 10.0 %collective-permute-start.20 = (f32[512]{0:T(512)}, f32[512]{0:T(512)}, u32[]{:S(2)}, u32[]{:S(2)}) collective-permute-start(f32[512]{0:T(512)} %param.16), channel_id=1, source_target_pairs={{0,1},{1,0},{2,3},{3,2},{4,5},{5,4},{6,7},{7,6},{8,9},{9,8},{10,11... | collective-permute-start | bytes 6152 | tf_op jit(solution)/shard_map/ppermute | solution.py:138
  21.4 19.2 %copy-start.1 = (bf16[256,4096]{1,0:T(8,128)(2,1)S(1)}, bf16[256,4096]{1,0:T(8,128)(2,1)}, u32[]{:S(2)}) copy-start(bf16[256,4096]{1,0:T(8,128)(2,1)} %param.22) | copy-start | bytes 6291460
  21.4 1.5 collective-permute-start.21
  22.9 16.2 %collective-permute-start.6 = (bf16[256,768]{1,0:T(8,128)(2,1)}, bf16[256,768]{1,0:T(8,128)(2,1)S(1)}, u32[]{:S(2)}, u32[]{:S(2)}) collective-permute-start(bf16[256,768]{1,0:T(8,128)(2,1)} %pad_maximum_fusion.5), channel_id=1, source_target_pairs={{0,12},{2,14},{4,8},{6,10},{8,4},{10,6},{12,0},{14,2},{1,13},{3,15... | collective-permute-start | bytes 1179656 | tf_op jit(solution)/shard_map/ppermute | solution.py:123
  23.8 14.2 %collective-permute-start.2 = (bf16[256,1024]{1,0:T(8,128)(2,1)}, bf16[256,1024]{1,0:T(8,128)(2,1)S(1)}, u32[]{:S(2)}, u32[]{:S(2)}) collective-permute-start(bf16[256,1024]{1,0:T(8,128)(2,1)} %constant_dynamic-slice_fusion.5), channel_id=1, source_target_pairs={{0,2},{2,0},{4,6},{6,4},{8,10},{10,8},{12,14},{14,12},{1,3},{3,1},... | collective-permute-start | bytes 1572872 | tf_op jit(solution)/shard_map/ppermute | solution.py:111
  27.5 15.2 %collective-permute-start.9 = (bf16[256,768]{1,0:T(8,128)(2,1)}, bf16[256,768]{1,0:T(8,128)(2,1)S(1)}, u32[]{:S(2)}, u32[]{:S(2)}) collective-permute-start(bf16[256,768]{1,0:T(8,128)(2,1)} %collective-permute-done), channel_id=1, source_target_pairs={{0,16},{16,0},{1,17},{17,1},{2,18},{18,2},{3,19},{19,3},{4,20},{20... | collective-permute-start | bytes 1179656 | tf_op jit(solution)/shard_map/ppermute | solution.py:108
  38.1 22.6 %collective-permute-start.3 = (bf16[256,768]{1,0:T(8,128)(2,1)S(1)}, bf16[256,768]{1,0:T(8,128)(2,1)S(1)}, u32[]{:S(2)}, u32[]{:S(2)}) collective-permute-start(bf16[256,768]{1,0:T(8,128)(2,1)S(1)} %collective-permute-done.1), channel_id=1, source_target_pairs={{0,2},{2,0},{4,6},{6,4},{8,10},{10,8},{12,14},{14,12},{1,3},{3,1},... | collective-permute-start | bytes 1179656 | tf_op jit(solution)/shard_map/ppermute | solution.py:111
  38.7 28.1 %collective-permute-start.11 = (bf16[256,768]{1,0:T(8,128)(2,1)S(1)}, bf16[256,768]{1,0:T(8,128)(2,1)S(1)}, u32[]{:S(2)}, u32[]{:S(2)}) collective-permute-start(bf16[256,768]{1,0:T(8,128)(2,1)S(1)} %collective-permute-done.1), channel_id=1, source_target_pairs={{0,16},{16,0},{1,17},{17,1},{2,18},{18,2},{3,19},{19,3},{4,20},{20... | collective-permute-start | bytes 1179656 | tf_op jit(solution)/shard_map/ppermute | solution.py:108
  39.1 19.4 %collective-permute-start.7 = (bf16[256,768]{1,0:T(8,128)(2,1)S(1)}, bf16[256,768]{1,0:T(8,128)(2,1)S(1)}, u32[]{:S(2)}, u32[]{:S(2)}) collective-permute-start(bf16[256,768]{1,0:T(8,128)(2,1)S(1)} %collective-permute-done.6), channel_id=1, source_target_pairs={{0,2},{2,0},{4,6},{6,4},{8,10},{10,8},{12,14},{14,12},{1,3},{3,1},... | collective-permute-start | bytes 1179656 | tf_op jit(solution)/shard_map/ppermute | solution.py:111
  41.1 17.9 %collective-permute-start.17 = (bf16[256,768]{1,0:T(8,128)(2,1)S(1)}, bf16[256,768]{1,0:T(8,128)(2,1)S(1)}, u32[]{:S(2)}, u32[]{:S(2)}) collective-permute-start(bf16[256,768]{1,0:T(8,128)(2,1)S(1)} %collective-permute-done.6), channel_id=1, source_target_pairs={{0,16},{16,0},{1,17},{17,1},{2,18},{18,2},{3,19},{19,3},{4,20},{20... | collective-permute-start | bytes 1179656 | tf_op jit(solution)/shard_map/ppermute | solution.py:108
  42.7 22.5 %collective-permute-start.5 = (bf16[256,768]{1,0:T(8,128)(2,1)S(1)}, bf16[256,768]{1,0:T(8,128)(2,1)S(1)}, u32[]{:S(2)}, u32[]{:S(2)}) collective-permute-start(bf16[256,768]{1,0:T(8,128)(2,1)S(1)} %collective-permute-done.4), channel_id=1, source_target_pairs={{0,2},{2,0},{4,6},{6,4},{8,10},{10,8},{12,14},{14,12},{1,3},{3,1},... | collective-permute-start | bytes 1179656 | tf_op jit(solution)/shard_map/ppermute | solution.py:111
  58.5 9.9 %collective-permute-start.14 = (bf16[256,768]{1,0:T(8,128)(2,1)S(1)}, bf16[256,768]{1,0:T(8,128)(2,1)S(1)}, u32[]{:S(2)}, u32[]{:S(2)}) collective-permute-start(bf16[256,768]{1,0:T(8,128)(2,1)S(1)} %collective-permute-done.4), channel_id=1, source_target_pairs={{0,16},{16,0},{1,17},{17,1},{2,18},{18,2},{3,19},{19,3},{4,20},{20... | collective-permute-start | bytes 1179656 | tf_op jit(solution)/shard_map/ppermute | solution.py:108
  59.0 68.7 %collective-permute-start.29 = (bf16[512,1024]{1,0:T(8,128)(2,1)S(1)}, bf16[512,1024]{1,0:T(8,128)(2,1)S(1)}, u32[]{:S(2)}, u32[]{:S(2)}) collective-permute-start(bf16[512,1024]{1,0:T(8,128)(2,1)S(1)} %pad_maximum_fusion.3), channel_id=1, source_target_pairs={{0,8},{2,10},{4,12},{6,14},{8,0},{10,2},{12,4},{14,6},{1,9},{3,11}... | collective-permute-start | bytes 3145736 | tf_op jit(solution)/shard_map/ppermute | solution.py:123
  60.6 28.7 %collective-permute-start.10 = (bf16[1536,512]{1,0:T(8,128)(2,1)S(1)}, bf16[1536,512]{1,0:T(8,128)(2,1)S(1)}, u32[]{:S(2)}, u32[]{:S(2)}) collective-permute-start(bf16[1536,512]{1,0:T(8,128)(2,1)S(1)} %maximum_dynamic-update-slice_fusion.4), channel_id=1, source_target_pairs={{0,1},{1,0},{2,3},{3,2},{4,5},{5,4},{6,7},{7,6},{8,9},{9,8},{10,11... | collective-permute-start | bytes 4718600 | tf_op jit(solution)/shard_map/ppermute | solution.py:138
  65.7 12.1 %collective-permute-start.12 = (bf16[256,768]{1,0:T(8,128)(2,1)S(1)}, bf16[256,768]{1,0:T(8,128)(2,1)S(1)}, u32[]{:S(2)}, u32[]{:S(2)}) collective-permute-start(bf16[256,768]{1,0:T(8,128)(2,1)S(1)} %collective-permute-done.3), channel_id=1, source_target_pairs={{0,16},{16,0},{1,17},{17,1},{2,18},{18,2},{3,19},{19,3},{4,20},{20... | collective-permute-start | bytes 1179656 | tf_op jit(solution)/shard_map/ppermute | solution.py:108
  66.8 16.8 %collective-permute-start.18 = (bf16[256,768]{1,0:T(8,128)(2,1)S(1)}, bf16[256,768]{1,0:T(8,128)(2,1)S(1)}, u32[]{:S(2)}, u32[]{:S(2)}) collective-permute-start(bf16[256,768]{1,0:T(8,128)(2,1)S(1)} %collective-permute-done.7), channel_id=1, source_target_pairs={{0,16},{16,0},{1,17},{17,1},{2,18},{18,2},{3,19},{19,3},{4,20},{20... | collective-permute-start | bytes 1179656 | tf_op jit(solution)/shard_map/ppermute | solution.py:108
  68.4 9.6 %collective-permute-start.15 = (bf16[256,768]{1,0:T(8,128)(2,1)S(1)}, bf16[256,768]{1,0:T(8,128)(2,1)S(1)}, u32[]{:S(2)}, u32[]{:S(2)}) collective-permute-start(bf16[256,768]{1,0:T(8,128)(2,1)S(1)} %collective-permute-done.14), channel_id=1, source_target_pairs={{0,2},{2,0},{4,6},{6,4},{8,10},{10,8},{12,14},{14,12},{1,3},{3,1},... | collective-permute-start | bytes 1179656 | tf_op jit(solution)/shard_map/ppermute | solution.py:111
  78.0 7.2 %collective-permute-start.13 = (bf16[1536,512]{1,0:T(8,128)(2,1)S(1)}, bf16[1536,512]{1,0:T(8,128)(2,1)S(1)}, u32[]{:S(2)}, u32[]{:S(2)}) collective-permute-start(bf16[1536,512]{1,0:T(8,128)(2,1)S(1)} %maximum_dynamic-update-slice_fusion.6), channel_id=1, source_target_pairs={{0,1},{1,0},{2,3},{3,2},{4,5},{5,4},{6,7},{7,6},{8,9},{9,8},{10,11... | collective-permute-start | bytes 4718600 | tf_op jit(solution)/shard_map/ppermute | solution.py:138
  78.3 8.4 %collective-permute-start.16 = (bf16[1536,512]{1,0:T(8,128)(2,1)S(1)}, bf16[1536,512]{1,0:T(8,128)(2,1)S(1)}, u32[]{:S(2)}, u32[]{:S(2)}) collective-permute-start(bf16[1536,512]{1,0:T(8,128)(2,1)S(1)} %maximum_dynamic-update-slice_fusion.8), channel_id=1, source_target_pairs={{0,1},{1,0},{2,3},{3,2},{4,5},{5,4},{6,7},{7,6},{8,9},{9,8},{10,11... | collective-permute-start | bytes 4718600 | tf_op jit(solution)/shard_map/ppermute | solution.py:138
  83.8 4.3 %collective-permute-start.19 = (bf16[1536,512]{1,0:T(8,128)(2,1)S(1)}, bf16[1536,512]{1,0:T(8,128)(2,1)S(1)}, u32[]{:S(2)}, u32[]{:S(2)}) collective-permute-start(bf16[1536,512]{1,0:T(8,128)(2,1)S(1)} %maximum_dynamic-update-slice_fusion.10), channel_id=1, source_target_pairs={{0,1},{1,0},{2,3},{3,2},{4,5},{5,4},{6,7},{7,6},{8,9},{9,8},{10,11... | collective-permute-start | bytes 4718600 | tf_op jit(solution)/shard_map/ppermute | solution.py:138
  85.1 41.2 %collective-permute-start.28 = (bf16[512,1024]{1,0:T(8,128)(2,1)S(1)}, bf16[512,1024]{1,0:T(8,128)(2,1)S(1)}, u32[]{:S(2)}, u32[]{:S(2)}) collective-permute-start(bf16[512,1024]{1,0:T(8,128)(2,1)S(1)} %pad_maximum_fusion.3), channel_id=1, source_target_pairs={{0,4},{2,6},{4,0},{6,2},{8,12},{10,14},{12,8},{14,10},{1,5},{3,7},... | collective-permute-start | bytes 3145736 | tf_op jit(solution)/shard_map/ppermute | solution.py:123
  86.6 78.1 %collective-permute-start.30 = (bf16[512,1024]{1,0:T(8,128)(2,1)S(1)}, bf16[512,1024]{1,0:T(8,128)(2,1)S(1)}, u32[]{:S(2)}, u32[]{:S(2)}) collective-permute-start(bf16[512,1024]{1,0:T(8,128)(2,1)S(1)} %pad_maximum_fusion.3), channel_id=1, source_target_pairs={{4,8},{6,10},{8,4},{10,6},{5,9},{7,11},{9,5},{11,7},{20,24},{22,26... | collective-permute-start | bytes 3145736 | tf_op jit(solution)/shard_map/ppermute | solution.py:123
  88.2 14.1 %collective-permute-start.32 = (bf16[1024,256]{1,0:T(8,128)(2,1)S(1)}, bf16[1024,256]{1,0:T(8,128)(2,1)S(1)}, u32[]{:S(2)}, u32[]{:S(2)}) collective-permute-start(bf16[1024,256]{1,0:T(8,128)(2,1)S(1)} %copy-done.2), channel_id=1, source_target_pairs={{0,2},{2,0},{4,6},{6,4},{8,10},{10,8},{12,14},{14,12},{1,3},{3,1},... | collective-permute-start | bytes 1572872 | tf_op jit(solution)/shard_map/ppermute | solution.py:111
  96.2 32.3 %collective-permute-start.22 = (bf16[128,2048]{1,0:T(8,128)(2,1)S(1)}, bf16[128,2048]{1,0:T(8,128)(2,1)S(1)}, u32[]{:S(2)}, u32[]{:S(2)}) collective-permute-start(bf16[128,2048]{1,0:T(8,128)(2,1)S(1)} %get-tuple-element.96), channel_id=1, source_target_pairs={{0,16},{16,0},{1,17},{17,1},{2,18},{18,2},{3,19},{19,3},{4,20},{20... | collective-permute-start | bytes 1572872 | tf_op jit(solution)/shard_map/ppermute | solution.py:108
  103.5 26.6 %collective-permute-start.23 = (bf16[128,2048]{1,0:T(8,128)(2,1)S(1)}, bf16[128,2048]{1,0:T(8,128)(2,1)S(1)}, u32[]{:S(2)}, u32[]{:S(2)}) collective-permute-start(bf16[128,2048]{1,0:T(8,128)(2,1)S(1)} %get-tuple-element.95), channel_id=1, source_target_pairs={{0,16},{16,0},{1,17},{17,1},{2,18},{18,2},{3,19},{19,3},{4,20},{20... | collective-permute-start | bytes 1572872 | tf_op jit(solution)/shard_map/ppermute | solution.py:108
  126.4 14.9 %collective-permute-start.24 = (bf16[128,2048]{1,0:T(8,128)(2,1)S(1)}, bf16[128,2048]{1,0:T(8,128)(2,1)S(1)}, u32[]{:S(2)}, u32[]{:S(2)}) collective-permute-start(bf16[128,2048]{1,0:T(8,128)(2,1)S(1)} %get-tuple-element.96), channel_id=1, source_target_pairs={{0,2},{2,0},{4,6},{6,4},{8,10},{10,8},{12,14},{14,12},{1,3},{3,1},... | collective-permute-start | bytes 1572872 | tf_op jit(solution)/shard_map/ppermute | solution.py:111
  127.7 24.8 %collective-permute-start.25 = (bf16[128,2048]{1,0:T(8,128)(2,1)S(1)}, bf16[128,2048]{1,0:T(8,128)(2,1)S(1)}, u32[]{:S(2)}, u32[]{:S(2)}) collective-permute-start(bf16[128,2048]{1,0:T(8,128)(2,1)S(1)} %get-tuple-element.95), channel_id=1, source_target_pairs={{0,2},{2,0},{4,6},{6,4},{8,10},{10,8},{12,14},{14,12},{1,3},{3,1},... | collective-permute-start | bytes 1572872 | tf_op jit(solution)/shard_map/ppermute | solution.py:111
  128.6 36.7 %collective-permute-start.31 = (bf16[512,1024]{1,0:T(8,128)(2,1)S(1)}, bf16[512,1024]{1,0:T(8,128)(2,1)S(1)}, u32[]{:S(2)}, u32[]{:S(2)}) collective-permute-start(bf16[512,1024]{1,0:T(8,128)(2,1)S(1)} %collective-permute-done.29), channel_id=1, source_target_pairs={{4,0},{6,2},{8,12},{10,14},{5,1},{7,3},{9,13},{11,15},{20,16},{22,... | collective-permute-start | bytes 3145736 | tf_op jit(solution)/shard_map/ppermute | solution.py:123
  130.2 32.7 %collective-permute-start.26 = (bf16[128,2048]{1,0:T(8,128)(2,1)S(1)}, bf16[128,2048]{1,0:T(8,128)(2,1)S(1)}, u32[]{:S(2)}, u32[]{:S(2)}) collective-permute-start(bf16[128,2048]{1,0:T(8,128)(2,1)S(1)} %collective-permute-done.22), channel_id=1, source_target_pairs={{0,2},{2,0},{4,6},{6,4},{8,10},{10,8},{12,14},{14,12},{1,3},{3,1},... | collective-permute-start | bytes 1572872 | tf_op jit(solution)/shard_map/ppermute | solution.py:111
  141.3 29.2 %collective-permute-start.33 = (bf16[512,1024]{1,0:T(8,128)(2,1)S(1)}, bf16[512,1024]{1,0:T(8,128)(2,1)S(1)}, u32[]{:S(2)}, u32[]{:S(2)}) collective-permute-start(bf16[512,1024]{1,0:T(8,128)(2,1)S(1)} %pad_maximum_fusion.3), channel_id=1, source_target_pairs={{0,1},{1,0},{2,3},{3,2},{4,5},{5,4},{6,7},{7,6},{8,9},{9,8},{10,11... | collective-permute-start | bytes 3145736 | tf_op jit(solution)/shard_map/ppermute | solution.py:138
  152.5 12.2 %collective-permute-start.27 = (bf16[128,2048]{1,0:T(8,128)(2,1)S(1)}, bf16[128,2048]{1,0:T(8,128)(2,1)S(1)}, u32[]{:S(2)}, u32[]{:S(2)}) collective-permute-start(bf16[128,2048]{1,0:T(8,128)(2,1)S(1)} %collective-permute-done.25), channel_id=1, source_target_pairs={{0,16},{16,0},{1,17},{17,1},{2,18},{18,2},{3,19},{19,3},{4,20},{20... | collective-permute-start | bytes 1572872 | tf_op jit(solution)/shard_map/ppermute | solution.py:108
  162.9 12.9 %collective-permute-start.37 = (bf16[1024,512]{1,0:T(8,128)(2,1)S(1)}, bf16[1024,512]{1,0:T(8,128)(2,1)S(1)}, u32[]{:S(2)}, u32[]{:S(2)}) collective-permute-start(bf16[1024,512]{1,0:T(8,128)(2,1)S(1)} %pad_maximum_fusion.4), channel_id=1, source_target_pairs={{0,1},{1,0},{2,3},{3,2},{4,5},{5,4},{6,7},{7,6},{8,9},{9,8},{10,11... | collective-permute-start | bytes 3145736 | tf_op jit(solution)/shard_map/ppermute | solution.py:138
  164.7 6.4 %collective-permute-start.34 = (bf16[512,1024]{1,0:T(8,128)(2,1)S(1)}, bf16[512,1024]{1,0:T(8,128)(2,1)S(1)}, u32[]{:S(2)}, u32[]{:S(2)}) collective-permute-start(bf16[512,1024]{1,0:T(8,128)(2,1)S(1)} %collective-permute-done.28), channel_id=1, source_target_pairs={{0,1},{1,0},{2,3},{3,2},{4,5},{5,4},{6,7},{7,6},{8,9},{9,8},{10,11... | collective-permute-start | bytes 3145736 | tf_op jit(solution)/shard_map/ppermute | solution.py:138
  164.7 6.3 %collective-permute-start.35 = (bf16[512,1024]{1,0:T(8,128)(2,1)S(1)}, bf16[512,1024]{1,0:T(8,128)(2,1)S(1)}, u32[]{:S(2)}, u32[]{:S(2)}) collective-permute-start(bf16[512,1024]{1,0:T(8,128)(2,1)S(1)} %collective-permute-done.29), channel_id=1, source_target_pairs={{0,1},{1,0},{2,3},{3,2},{4,5},{5,4},{6,7},{7,6},{8,9},{9,8},{10,11... | collective-permute-start | bytes 3145736 | tf_op jit(solution)/shard_map/ppermute | solution.py:138
  165.7 5.4 %collective-permute-start.36 = (bf16[512,1024]{1,0:T(8,128)(2,1)S(1)}, bf16[512,1024]{1,0:T(8,128)(2,1)S(1)}, u32[]{:S(2)}, u32[]{:S(2)}) collective-permute-start(bf16[512,1024]{1,0:T(8,128)(2,1)S(1)} %get-tuple-element.34), channel_id=1, source_target_pairs={{0,1},{1,0},{2,3},{3,2},{4,5},{5,4},{6,7},{7,6},{8,9},{9,8},{10,11... | collective-permute-start | bytes 3145736 | tf_op jit(solution)/shard_map/ppermute | solution.py:138
  170.5 78.3 %copy-start.20 = (bf16[1024,1024]{1,0:T(8,128)(2,1)}, bf16[1024,1024]{1,0:T(8,128)(2,1)S(1)}, u32[]{:S(2)}) copy-start(bf16[1024,1024]{1,0:T(8,128)(2,1)S(1)} %multiply_convert_fusion.1) | copy-start | bytes 6291460
  170.5 48.7 %collective-permute-start.42 = (bf16[1024,512]{1,0:T(8,128)(2,1)S(1)}, bf16[1024,512]{1,0:T(8,128)(2,1)S(1)}, u32[]{:S(2)}, u32[]{:S(2)}) collective-permute-start(bf16[1024,512]{1,0:T(8,128)(2,1)S(1)} %pad_maximum_fusion.4), channel_id=1, source_target_pairs={{0,8},{2,10},{4,12},{6,14},{8,0},{10,2},{12,4},{14,6},{1,9},{3,11}... | collective-permute-start | bytes 3145736 | tf_op jit(solution)/shard_map/ppermute | solution.py:123
  175.8 71.7 %copy-start.18 = (bf16[1024,1024]{1,0:T(8,128)(2,1)}, bf16[1024,1024]{1,0:T(8,128)(2,1)S(1)}, u32[]{:S(2)}) copy-start(bf16[1024,1024]{1,0:T(8,128)(2,1)S(1)} %multiply_convert_fusion) | copy-start | bytes 6291460
  178.4 9.2 %collective-permute-start.38 = (bf16[256,512]{1,0:T(8,128)(2,1)S(1)}, bf16[256,512]{1,0:T(8,128)(2,1)S(1)}, u32[]{:S(2)}, u32[]{:S(2)}) collective-permute-start(bf16[256,512]{1,0:T(8,128)(2,1)S(1)} %get-tuple-element.92), channel_id=1, source_target_pairs={{0,16},{16,0},{1,17},{17,1},{2,18},{18,2},{3,19},{19,3},{4,20},{20... | collective-permute-start | bytes 786440 | tf_op jit(solution)/shard_map/ppermute | solution.py:108
  179.9 13.7 %collective-permute-start.39 = (bf16[256,512]{1,0:T(8,128)(2,1)S(1)}, bf16[256,512]{1,0:T(8,128)(2,1)S(1)}, u32[]{:S(2)}, u32[]{:S(2)}) collective-permute-start(bf16[256,512]{1,0:T(8,128)(2,1)S(1)} %get-tuple-element.94), channel_id=1, source_target_pairs={{0,2},{2,0},{4,6},{6,4},{8,10},{10,8},{12,14},{14,12},{1,3},{3,1},... | collective-permute-start | bytes 786440 | tf_op jit(solution)/shard_map/ppermute | solution.py:111
  180.5 13.2 %collective-permute-start.40 = (bf16[256,512]{1,0:T(8,128)(2,1)S(1)}, bf16[256,512]{1,0:T(8,128)(2,1)S(1)}, u32[]{:S(2)}, u32[]{:S(2)}) collective-permute-start(bf16[256,512]{1,0:T(8,128)(2,1)S(1)} %get-tuple-element.93), channel_id=1, source_target_pairs={{0,18},{2,16},{4,22},{6,20},{8,26},{10,24},{12,30},{14,28},{16,2},... | collective-permute-start | bytes 786440 | tf_op jit(solution)/shard_map/ppermute | solution.py:119
  219.3 2.7 collective-permute-start.43
  219.4 25.5 %collective-permute-start.48 = (bf16[1024,512]{1,0:T(8,128)(2,1)S(1)}, bf16[1024,512]{1,0:T(8,128)(2,1)S(1)}, u32[]{:S(2)}, u32[]{:S(2)}) collective-permute-start(bf16[1024,512]{1,0:T(8,128)(2,1)S(1)} %pad_maximum_fusion.4), channel_id=1, source_target_pairs={{0,4},{2,6},{4,0},{6,2},{8,12},{10,14},{12,8},{14,10},{1,5},{3,7},... | collective-permute-start | bytes 3145736 | tf_op jit(solution)/shard_map/ppermute | solution.py:123
  224.5 9.2 %collective-permute-start.44 = (bf16[256,512]{1,0:T(8,128)(2,1)S(1)}, bf16[256,512]{1,0:T(8,128)(2,1)S(1)}, u32[]{:S(2)}, u32[]{:S(2)}) collective-permute-start(bf16[256,512]{1,0:T(8,128)(2,1)S(1)} %get-tuple-element.89), channel_id=1, source_target_pairs={{0,16},{16,0},{1,17},{17,1},{2,18},{18,2},{3,19},{19,3},{4,20},{20... | collective-permute-start | bytes 786440 | tf_op jit(solution)/shard_map/ppermute | solution.py:108
  226.1 13.7 %collective-permute-start.45 = (bf16[256,512]{1,0:T(8,128)(2,1)S(1)}, bf16[256,512]{1,0:T(8,128)(2,1)S(1)}, u32[]{:S(2)}, u32[]{:S(2)}) collective-permute-start(bf16[256,512]{1,0:T(8,128)(2,1)S(1)} %get-tuple-element.91), channel_id=1, source_target_pairs={{0,2},{2,0},{4,6},{6,4},{8,10},{10,8},{12,14},{14,12},{1,3},{3,1},... | collective-permute-start | bytes 786440 | tf_op jit(solution)/shard_map/ppermute | solution.py:111
  226.6 13.2 %collective-permute-start.46 = (bf16[256,512]{1,0:T(8,128)(2,1)S(1)}, bf16[256,512]{1,0:T(8,128)(2,1)S(1)}, u32[]{:S(2)}, u32[]{:S(2)}) collective-permute-start(bf16[256,512]{1,0:T(8,128)(2,1)S(1)} %get-tuple-element.90), channel_id=1, source_target_pairs={{0,18},{2,16},{4,22},{6,20},{8,26},{10,24},{12,30},{14,28},{16,2},... | collective-permute-start | bytes 786440 | tf_op jit(solution)/shard_map/ppermute | solution.py:119
  244.9 2.7 collective-permute-start.49
  244.9 28.2 %collective-permute-start.54 = (bf16[1024,512]{1,0:T(8,128)(2,1)S(1)}, bf16[1024,512]{1,0:T(8,128)(2,1)S(1)}, u32[]{:S(2)}, u32[]{:S(2)}) collective-permute-start(bf16[1024,512]{1,0:T(8,128)(2,1)S(1)} %pad_maximum_fusion.4), channel_id=1, source_target_pairs={{4,8},{6,10},{8,4},{10,6},{5,9},{7,11},{9,5},{11,7},{20,24},{22,26... | collective-permute-start | bytes 3145736 | tf_op jit(solution)/shard_map/ppermute | solution.py:123
  245.6 27.5 %collective-permute-start.55 = (bf16[1024,512]{1,0:T(8,128)(2,1)S(1)}, bf16[1024,512]{1,0:T(8,128)(2,1)S(1)}, u32[]{:S(2)}, u32[]{:S(2)}) collective-permute-start(bf16[1024,512]{1,0:T(8,128)(2,1)S(1)} %collective-permute-done.42), channel_id=1, source_target_pairs={{4,0},{6,2},{8,12},{10,14},{5,1},{7,3},{9,13},{11,15},{20,16},{22,... | collective-permute-start | bytes 3145736 | tf_op jit(solution)/shard_map/ppermute | solution.py:123
  250.1 9.2 %collective-permute-start.50 = (bf16[256,512]{1,0:T(8,128)(2,1)S(1)}, bf16[256,512]{1,0:T(8,128)(2,1)S(1)}, u32[]{:S(2)}, u32[]{:S(2)}) collective-permute-start(bf16[256,512]{1,0:T(8,128)(2,1)S(1)} %get-tuple-element.86), channel_id=1, source_target_pairs={{0,16},{16,0},{1,17},{17,1},{2,18},{18,2},{3,19},{19,3},{4,20},{20... | collective-permute-start | bytes 786440 | tf_op jit(solution)/shard_map/ppermute | solution.py:108
  251.6 13.7 %collective-permute-start.51 = (bf16[256,512]{1,0:T(8,128)(2,1)S(1)}, bf16[256,512]{1,0:T(8,128)(2,1)S(1)}, u32[]{:S(2)}, u32[]{:S(2)}) collective-permute-start(bf16[256,512]{1,0:T(8,128)(2,1)S(1)} %get-tuple-element.88), channel_id=1, source_target_pairs={{0,2},{2,0},{4,6},{6,4},{8,10},{10,8},{12,14},{14,12},{1,3},{3,1},... | collective-permute-start | bytes 786440 | tf_op jit(solution)/shard_map/ppermute | solution.py:111
  252.2 13.2 %collective-permute-start.52 = (bf16[256,512]{1,0:T(8,128)(2,1)S(1)}, bf16[256,512]{1,0:T(8,128)(2,1)S(1)}, u32[]{:S(2)}, u32[]{:S(2)}) collective-permute-start(bf16[256,512]{1,0:T(8,128)(2,1)S(1)} %get-tuple-element.87), channel_id=1, source_target_pairs={{0,18},{2,16},{4,22},{6,20},{8,26},{10,24},{12,30},{14,28},{16,2},... | collective-permute-start | bytes 786440 | tf_op jit(solution)/shard_map/ppermute | solution.py:119
  273.2 3.7 %collective-permute-start.56 = (bf16[1024,512]{1,0:T(8,128)(2,1)S(1)}, bf16[1024,512]{1,0:T(8,128)(2,1)}, u32[]{:S(2)}, u32[]{:S(2)}) collective-permute-start(bf16[1024,512]{1,0:T(8,128)(2,1)S(1)} %broadcast_select_fusion), channel_id=1, source_target_pairs={{0,1},{1,0},{2,3},{3,2},{4,5},{5,4},{6,7},{7,6},{8,9},{9,8},{10,11... | collective-permute-start | bytes 3145736 | tf_op jit(solution)/shard_map/ppermute | solution.py:138
  273.2 3.0 %collective-permute-start.41 = (bf16[256,512]{1,0:T(8,128)(2,1)S(1)}, bf16[256,512]{1,0:T(8,128)(2,1)S(1)}, u32[]{:S(2)}, u32[]{:S(2)}) collective-permute-start(bf16[256,512]{1,0:T(8,128)(2,1)S(1)} %add_convert_fusion.8), channel_id=1, source_target_pairs={{0,1},{1,0},{2,3},{3,2},{4,5},{5,4},{6,7},{7,6},{8,9},{9,8},{10,11... | collective-permute-start | bytes 786440 | tf_op jit(solution)/shard_map/ppermute | solution.py:138
  276.6 7.7 %collective-permute-start.47 = (bf16[256,512]{1,0:T(8,128)(2,1)S(1)}, bf16[256,512]{1,0:T(8,128)(2,1)S(1)}, u32[]{:S(2)}, u32[]{:S(2)}) collective-permute-start(bf16[256,512]{1,0:T(8,128)(2,1)S(1)} %add_convert_fusion.7), channel_id=1, source_target_pairs={{0,1},{1,0},{2,3},{3,2},{4,5},{5,4},{6,7},{7,6},{8,9},{9,8},{10,11... | collective-permute-start | bytes 786440 | tf_op jit(solution)/shard_map/ppermute | solution.py:138
  280.8 9.2 %collective-permute-start.57 = (bf16[256,512]{1,0:T(8,128)(2,1)S(1)}, bf16[256,512]{1,0:T(8,128)(2,1)S(1)}, u32[]{:S(2)}, u32[]{:S(2)}) collective-permute-start(bf16[256,512]{1,0:T(8,128)(2,1)S(1)} %get-tuple-element.83), channel_id=1, source_target_pairs={{0,16},{16,0},{1,17},{17,1},{2,18},{18,2},{3,19},{19,3},{4,20},{20... | collective-permute-start | bytes 786440 | tf_op jit(solution)/shard_map/ppermute | solution.py:108
  282.3 14.0 %collective-permute-start.58 = (bf16[256,512]{1,0:T(8,128)(2,1)S(1)}, bf16[256,512]{1,0:T(8,128)(2,1)S(1)}, u32[]{:S(2)}, u32[]{:S(2)}) collective-permute-start(bf16[256,512]{1,0:T(8,128)(2,1)S(1)} %get-tuple-element.85), channel_id=1, source_target_pairs={{0,2},{2,0},{4,6},{6,4},{8,10},{10,8},{12,14},{14,12},{1,3},{3,1},... | collective-permute-start | bytes 786440 | tf_op jit(solution)/shard_map/ppermute | solution.py:111
  282.8 13.5 %collective-permute-start.59 = (bf16[256,512]{1,0:T(8,128)(2,1)S(1)}, bf16[256,512]{1,0:T(8,128)(2,1)S(1)}, u32[]{:S(2)}, u32[]{:S(2)}) collective-permute-start(bf16[256,512]{1,0:T(8,128)(2,1)S(1)} %get-tuple-element.84), channel_id=1, source_target_pairs={{0,18},{2,16},{4,22},{6,20},{8,26},{10,24},{12,30},{14,28},{16,2},... | collective-permute-start | bytes 786440 | tf_op jit(solution)/shard_map/ppermute | solution.py:119
  284.4 12.2 %collective-permute-start.53 = (bf16[256,512]{1,0:T(8,128)(2,1)S(1)}, bf16[256,512]{1,0:T(8,128)(2,1)S(1)}, u32[]{:S(2)}, u32[]{:S(2)}) collective-permute-start(bf16[256,512]{1,0:T(8,128)(2,1)S(1)} %add_convert_fusion.6), channel_id=1, source_target_pairs={{0,1},{1,0},{2,3},{3,2},{4,5},{5,4},{6,7},{7,6},{8,9},{9,8},{10,11... | collective-permute-start | bytes 786440 | tf_op jit(solution)/shard_map/ppermute | solution.py:138
  296.5 1.6 collective-permute-start.60
  (19 other events, 58.4 us)
where the time goes:
time: 300 us; the launch traced here: 299 us
  waiting for transfers between devices  192 us (64%)
  starting transfers between devices  51 us (17%)
  matrix products  29.1 us (10%)
  other arithmetic  15.4 us (5%)
  local copies, waits for them, and re-layouts  10.6 us (4%)
    ppermute x14, waiting for transfers between devices, over_y(): return lax.ppermute(a, 'fs', [(i, i ^ 1) for i in range(shards)])  87.6 us
    ppermute x11, waiting for transfers between devices, over_z(): lax.ppermute(a, 'fs', [p for p in pairs if layers is None or p[0] // SIDE...  59.1 us
    ppermute x14, waiting for transfers between devices, over_x(): return lax.ppermute(a, 'rep', [(i, reps - 1 - i) for i in range(reps)])  37.9 us
    dot_general x38, matrix products, dot(): return jnp.dot(a, b, preferred_element_type=f32)  29.1 us
    ppermute x14, starting transfers between devices, over_x(): return lax.ppermute(a, 'rep', [(i, reps - 1 - i) for i in range(reps)])  17.4 us
    ppermute x11, starting transfers between devices, over_z(): lax.ppermute(a, 'fs', [p for p in pairs if layers is None or p[0] // SIDE...  13.6 us
    ppermute x14, starting transfers between devices, over_y(): return lax.ppermute(a, 'fs', [(i, i ^ 1) for i in range(shards)])  11.3 us
    ppermute x18, waiting for transfers between devices, over_core(): return lax.ppermute(a, 'tp', [(i, cores - 1 - i) for i in range(cores)])  7.11 us
  transfers between devices with their start and end apart: 61, of which 28 were waited for; matrix products, arithmetic and copies ran while one was open for 17% of the time, Pallas kernels for 0%

commit v1 on v0

--- a/solution.py
+++ b/solution.py
@@ -273,11 +273,15 @@
         elif k == 1:
             mine = after(down_first, total)
         else:
-            mine = jnp.where(inner, down_third, after(down_relayed, total))
+            mine = jnp.where(inner, down_third, after(down_relayed, arrived[0]))
         part = (dot(hidden[0], mine) + dot(hidden[1], over_core(mine))).astype(bf16)
         total = part[:rows].astype(f32)
-        for n, send in enumerate((over_x, over_y, over_xy)):
-            total = total + send(part[(n + 1) * rows : (n + 2) * rows]).astype(f32)
+        arrived = [
+            send(part[(n + 1) * rows : (n + 2) * rows])
+            for n, send in enumerate((over_x, over_y, over_xy))
+        ]
+        for term in arrived:
+            total = total + term.astype(f32)
         final = (midway[:, k * width : (k + 1) * width].astype(f32) + total).astype(bf16)
         sibling = over_core(final)
         both = jnp.concatenate(

time: 300 us -> 305 us (1.017)
    ppermute x11, waiting for transfers between devices: 59.1 us -> 71.9 us  [over_z(): lax.ppermute(a, 'fs', [p for p in pairs if layers is None or p[0] // SIDE...]
    ppermute x14, waiting for transfers between devices: 37.9 us -> 28.3 us  [over_x(): return lax.ppermute(a, 'rep', [(i, reps - 1 - i) for i in range(reps)])]
  transfers between devices with their start and end apart: 61 -> 61, of which waited for: 28 -> 27; matrix products, arithmetic and copies ran while one was open for 17% -> 17% of each run, Pallas kernels for 0% -> 0%
where the time goes in v1:
time: 305 us; the launch traced here: 304 us
  waiting for transfers between devices  192 us (63%)
  starting transfers between devices  52 us (17%)
  matrix products  29.6 us (10%)
  other arithmetic  16.1 us (5%)
  local copies, waits for them, and re-layouts  13.1 us (4%)
    ppermute x14, waiting for transfers between devices, over_y(): return lax.ppermute(a, 'fs', [(i, i ^ 1) for i in range(shards)])  87.5 us
    ppermute x11, waiting for transfers between devices, over_z(): lax.ppermute(a, 'fs', [p for p in pairs if layers is None or p[0] // SIDE...  71.9 us
    dot_general x38, matrix products, dot(): return jnp.dot(a, b, preferred_element_type=f32)  29.6 us
    ppermute x14, waiting for transfers between devices, over_x(): return lax.ppermute(a, 'rep', [(i, reps - 1 - i) for i in range(reps)])  28.3 us
    ppermute x14, starting transfers between devices, over_x(): return lax.ppermute(a, 'rep', [(i, reps - 1 - i) for i in range(reps)])  16.3 us
    ppermute x11, starting transfers between devices, over_z(): lax.ppermute(a, 'fs', [p for p in pairs if layers is None or p[0] // SIDE...  13.6 us
    ppermute x14, starting transfers between devices, over_y(): return lax.ppermute(a, 'fs', [(i, i ^ 1) for i in range(shards)])  13.1 us
  transfers between devices with their start and end apart: 61, of which 27 were waited for; matrix products, arithmetic and copies ran while one was open for 17% of the time, Pallas kernels for 0%

profile of v1, /device:TPU:0, one launch (start us, length us, event | category | flops | bytes accessed | tf_op | source)
XLA Modules:
  0.0 304.0 jit_solution(10182367314420872592)
XLA Ops:
  2.7 3.1 %collective-permute-start.1 = (bf16[256,768]{1,0:T(8,128)(2,1)}, bf16[256,768]{1,0:T(8,128)(2,1)S(1)}, u32[]{:S(2)}, u32[]{:S(2)}) collective-permute-start(bf16[256,768]{1,0:T(8,128)(2,1)} %pad_maximum_fusion.5), channel_id=1, source_target_pairs={{0,4},{2,6},{4,0},{6,2},{8,12},{10,14},{12,8},{14,10},{1,5},{3,7},... | collective-permute-start | bytes 1179656 | tf_op jit(solution)/shard_map/ppermute | solution.py:123
  5.8 1.5 collective-permute-start
  7.3 1.5 collective-permute-start.8
  8.8 2.6 collective-permute-start.4
  11.4 2.0 fusion.177
  14.9 1.9 constant_dynamic-slice_fusion.5
  16.8 1.9 constant_dynamic-slice_fusion
  24.3 1.0 constant_dynamic-update-slice_fusion.3
  25.3 1.0 broadcast_select_fusion.46
  26.4 1.0 constant_dynamic-update-slice_fusion.2
  27.8 10.2 %collective-permute-done.2 = bf16[256,1024]{1,0:T(8,128)(2,1)S(1)} collective-permute-done((bf16[256,1024]{1,0:T(8,128)(2,1)}, bf16[256,1024]{1,0:T(8,128)(2,1)S(1)}, u32[]{:S(2)}, u32[]{:S(2)}) %collective-permute-start.2) | collective-permute-done | bytes 524320 | tf_op jit(solution)/shard_map/ppermute | solution.py:111
  39.0 1.5 collective-permute-start.7
  41.0 1.6 collective-permute-start.17
  43.6 14.8 %collective-permute-done.7 = bf16[256,768]{1,0:T(8,128)(2,1)S(1)} collective-permute-done((bf16[256,768]{1,0:T(8,128)(2,1)S(1)}, bf16[256,768]{1,0:T(8,128)(2,1)S(1)}, u32[]{:S(2)}, u32[]{:S(2)}) %collective-permute-start.7) | collective-permute-done | bytes 393248 | tf_op jit(solution)/shard_map/ppermute | solution.py:111
  58.9 1.6 collective-permute-start.29
  61.3 3.8 %collective-permute-done.5 = bf16[256,768]{1,0:T(8,128)(2,1)S(1)} collective-permute-done((bf16[256,768]{1,0:T(8,128)(2,1)S(1)}, bf16[256,768]{1,0:T(8,128)(2,1)S(1)}, u32[]{:S(2)}, u32[]{:S(2)}) %collective-permute-start.5) | collective-permute-done | bytes 393248 | tf_op jit(solution)/shard_map/ppermute | solution.py:111
  66.7 1.6 collective-permute-start.18
  68.8 8.8 %collective-permute-done.12 = bf16[256,768]{1,0:T(8,128)(2,1)S(1)} collective-permute-done((bf16[256,768]{1,0:T(8,128)(2,1)S(1)}, bf16[256,768]{1,0:T(8,128)(2,1)S(1)}, u32[]{:S(2)}, u32[]{:S(2)}) %collective-permute-start.12) | collective-permute-done | bytes 393248 | tf_op jit(solution)/shard_map/ppermute | solution.py:108
  78.7 4.8 %collective-permute-done.18 = bf16[256,768]{1,0:T(8,128)(2,1)S(1)} collective-permute-done((bf16[256,768]{1,0:T(8,128)(2,1)S(1)}, bf16[256,768]{1,0:T(8,128)(2,1)S(1)}, u32[]{:S(2)}, u32[]{:S(2)}) %collective-permute-start.18) | collective-permute-done | bytes 393248 | tf_op jit(solution)/shard_map/ppermute | solution.py:108
  96.1 1.6 collective-permute-start.22
  97.7 4.5 %collective-permute-done.32 = bf16[1024,256]{1,0:T(8,128)(2,1)S(1)} collective-permute-done((bf16[1024,256]{1,0:T(8,128)(2,1)S(1)}, bf16[1024,256]{1,0:T(8,128)(2,1)S(1)}, u32[]{:S(2)}, u32[]{:S(2)}) %collective-permute-start.32) | collective-permute-done | bytes 524320 | tf_op jit(solution)/shard_map/ppermute | solution.py:111
  102.2 1.2 broadcast_select_fusion.3
  103.5 1.5 collective-permute-start.23
  105.1 21.2 %collective-permute-done.28 = bf16[512,1024]{1,0:T(8,128)(2,1)S(1)} collective-permute-done((bf16[512,1024]{1,0:T(8,128)(2,1)S(1)}, bf16[512,1024]{1,0:T(8,128)(2,1)S(1)}, u32[]{:S(2)}, u32[]{:S(2)}) %collective-permute-start.28) | collective-permute-done | bytes 1048608 | tf_op jit(solution)/shard_map/ppermute | solution.py:123
  126.3 1.3 collective-permute-start.24
  128.5 1.5 collective-permute-start.31
  130.1 1.3 collective-permute-start.26
  131.4 9.8 %collective-permute-done.24 = bf16[128,2048]{1,0:T(8,128)(2,1)S(1)} collective-permute-done((bf16[128,2048]{1,0:T(8,128)(2,1)S(1)}, bf16[128,2048]{1,0:T(8,128)(2,1)S(1)}, u32[]{:S(2)}, u32[]{:S(2)}) %collective-permute-start.24) | collective-permute-done | bytes 524320 | tf_op jit(solution)/shard_map/ppermute | solution.py:111
  141.2 11.2 %collective-permute-done.25 = bf16[128,2048]{1,0:T(8,128)(2,1)S(1)} collective-permute-done((bf16[128,2048]{1,0:T(8,128)(2,1)S(1)}, bf16[128,2048]{1,0:T(8,128)(2,1)S(1)}, u32[]{:S(2)}, u32[]{:S(2)}) %collective-permute-start.25) | collective-permute-done | bytes 524320 | tf_op jit(solution)/shard_map/ppermute | solution.py:111
  152.4 1.5 collective-permute-start.27
  154.0 8.8 %collective-permute-done.26 = bf16[128,2048]{1,0:T(8,128)(2,1)S(1)} collective-permute-done((bf16[128,2048]{1,0:T(8,128)(2,1)S(1)}, bf16[128,2048]{1,0:T(8,128)(2,1)S(1)}, u32[]{:S(2)}, u32[]{:S(2)}) %collective-permute-start.26) | collective-permute-done | bytes 524320 | tf_op jit(solution)/shard_map/ppermute | solution.py:111
  162.8 1.8 collective-permute-done.27
  165.7 4.7 %multiply_convert_fusion.1 = bf16[1024,1024]{1,0:T(8,128)(2,1)S(1)} fusion(bf16[1024,2048]{1,0:T(8,128)(2,1)S(1)} %constant_dynamic-update-slice_fusion.16, bf16[2048,1024]{1,0:T(8,128)(2,1)S(1)} %get-tuple-element.31), kind=kOutput, calls=%fused_computation.9 | convolution fusion | flops 4298113024 | bytes 10485760 | tf_op jit(solution)/shard_map/dot_general | solution.py:149
  171.0 4.7 %multiply_convert_fusion = bf16[1024,1024]{1,0:T(8,128)(2,1)S(1)} fusion(bf16[1024,2048]{1,0:T(8,128)(2,1)S(1)} %constant_dynamic-update-slice_fusion.16, bf16[512,1024]{1,0:T(8,128)(2,1)S(1)} %collective-permute-done.36, bf16[512,1024]{1,0:T(8,128)(2,1)S(1)} %collective-permute-done.35, bf16[512,1024]{1,0:T(8,128)(2,1)S(1)} %collective-permute-done.34, ...), kind=kOutput, calls=%fused_computation.8 | convolution fusion | flops 4314890240 | bytes 10485760 | tf_op jit(solution)/shard_map/dot_general | solution.py:149
  175.8 1.2 fusion.185
  177.0 1.3 add_convert_fusion.3
  178.3 1.5 collective-permute-start.38
  180.4 1.4 collective-permute-start.40
  181.9 5.7 %collective-permute-done.38 = bf16[256,512]{1,0:T(8,128)(2,1)S(1)} collective-permute-done((bf16[256,512]{1,0:T(8,128)(2,1)S(1)}, bf16[256,512]{1,0:T(8,128)(2,1)S(1)}, u32[]{:S(2)}, u32[]{:S(2)}) %collective-permute-start.38) | collective-permute-done | bytes 262176 | tf_op jit(solution)/shard_map/ppermute | solution.py:108
  187.6 6.0 %collective-permute-done.39 = bf16[256,512]{1,0:T(8,128)(2,1)S(1)} collective-permute-done((bf16[256,512]{1,0:T(8,128)(2,1)S(1)}, bf16[256,512]{1,0:T(8,128)(2,1)S(1)}, u32[]{:S(2)}, u32[]{:S(2)}) %collective-permute-start.39) | collective-permute-done | bytes 262176 | tf_op jit(solution)/shard_map/ppermute | solution.py:111
  194.5 24.8 %collective-permute-done.42 = bf16[1024,512]{1,0:T(8,128)(2,1)S(1)} collective-permute-done((bf16[1024,512]{1,0:T(8,128)(2,1)S(1)}, bf16[1024,512]{1,0:T(8,128)(2,1)S(1)}, u32[]{:S(2)}, u32[]{:S(2)}) %collective-permute-start.42) | collective-permute-done | bytes 1048608 | tf_op jit(solution)/shard_map/ppermute | solution.py:123
  219.3 2.6 collective-permute-done.43
  221.9 1.2 fusion.186
  223.1 1.2 add_convert_fusion.2
  224.5 1.5 collective-permute-start.44
  226.6 1.4 collective-permute-start.46
  228.0 5.7 %collective-permute-done.44 = bf16[256,512]{1,0:T(8,128)(2,1)S(1)} collective-permute-done((bf16[256,512]{1,0:T(8,128)(2,1)S(1)}, bf16[256,512]{1,0:T(8,128)(2,1)S(1)}, u32[]{:S(2)}, u32[]{:S(2)}) %collective-permute-start.44) | collective-permute-done | bytes 262176 | tf_op jit(solution)/shard_map/ppermute | solution.py:108
  233.7 5.9 %collective-permute-done.45 = bf16[256,512]{1,0:T(8,128)(2,1)S(1)} collective-permute-done((bf16[256,512]{1,0:T(8,128)(2,1)S(1)}, bf16[256,512]{1,0:T(8,128)(2,1)S(1)}, u32[]{:S(2)}, u32[]{:S(2)}) %collective-permute-start.45) | collective-permute-done | bytes 262176 | tf_op jit(solution)/shard_map/ppermute | solution.py:111
  239.8 5.0 %collective-permute-done.48 = bf16[1024,512]{1,0:T(8,128)(2,1)S(1)} collective-permute-done((bf16[1024,512]{1,0:T(8,128)(2,1)S(1)}, bf16[1024,512]{1,0:T(8,128)(2,1)S(1)}, u32[]{:S(2)}, u32[]{:S(2)}) %collective-permute-start.48) | collective-permute-done | bytes 1048608 | tf_op jit(solution)/shard_map/ppermute | solution.py:123
  245.5 1.6 collective-permute-start.55
  247.5 1.2 fusion.187
  248.7 1.2 add_convert_fusion.1
  250.9 1.4 collective-permute-start.50
  252.3 20.7 %collective-permute-done.55 = bf16[1024,512]{1,0:T(8,128)(2,1)S(1)} collective-permute-done((bf16[1024,512]{1,0:T(8,128)(2,1)S(1)}, bf16[1024,512]{1,0:T(8,128)(2,1)S(1)}, u32[]{:S(2)}, u32[]{:S(2)}) %collective-permute-start.55) | collective-permute-done | bytes 1048608 | tf_op jit(solution)/shard_map/ppermute | solution.py:123
  274.4 1.4 collective-permute-start.51
  275.8 1.5 collective-permute-start.52
  277.3 3.1 %fusion.188 = f32[1024,512]{1,0:T(8,128)S(1)} fusion(bf16[1024,1024]{1,0:T(8,128)(2,1)} %copy-done.21, bf16[1024,512]{1,0:T(8,128)(2,1)} %collective-permute-done.56), kind=kOutput, calls=%fused_computation.349 | convolution fusion | flops 1073741824 | bytes 5242880 | tf_op jit(solution)/shard_map/dot_general | solution.py:149
  280.4 1.2 add_convert_fusion
  282.6 1.2 collective-permute-start.58
  283.8 1.5 collective-permute-start.59
  285.7 3.7 %collective-permute-done.51 = bf16[256,512]{1,0:T(8,128)(2,1)S(1)} collective-permute-done((bf16[256,512]{1,0:T(8,128)(2,1)}, bf16[256,512]{1,0:T(8,128)(2,1)S(1)}, u32[]{:S(2)}, u32[]{:S(2)}) %collective-permute-start.51) | collective-permute-done | bytes 262176 | tf_op jit(solution)/shard_map/ppermute | solution.py:111
  289.4 1.6 collective-permute-done.57
  291.0 8.8 %collective-permute-done.58 = bf16[256,512]{1,0:T(8,128)(2,1)S(1)} collective-permute-done((bf16[256,512]{1,0:T(8,128)(2,1)S(1)}, bf16[256,512]{1,0:T(8,128)(2,1)S(1)}, u32[]{:S(2)}, u32[]{:S(2)}) %collective-permute-start.58) | collective-permute-done | bytes 262176 | tf_op jit(solution)/shard_map/ppermute | solution.py:111
  302.2 1.0 copy-done
  (238 shorter events, 42.5 us)
Async XLA Ops:
  2.7 24.7 %collective-permute-start.1 = (bf16[256,768]{1,0:T(8,128)(2,1)}, bf16[256,768]{1,0:T(8,128)(2,1)S(1)}, u32[]{:S(2)}, u32[]{:S(2)}) collective-permute-start(bf16[256,768]{1,0:T(8,128)(2,1)} %pad_maximum_fusion.5), channel_id=1, source_target_pairs={{0,4},{2,6},{4,0},{6,2},{8,12},{10,14},{12,8},{14,10},{1,5},{3,7},... | collective-permute-start | bytes 1179656 | tf_op jit(solution)/shard_map/ppermute | solution.py:123
  5.8 18.0 %collective-permute-start = (bf16[256,768]{1,0:T(8,128)(2,1)}, bf16[256,768]{1,0:T(8,128)(2,1)}, u32[]{:S(2)}, u32[]{:S(2)}) collective-permute-start(bf16[256,768]{1,0:T(8,128)(2,1)} %pad_maximum_fusion.5), channel_id=1, source_target_pairs={{0,2},{2,0},{4,6},{6,4},{8,10},{10,8},{12,14},{14,12},{1,3},{3,1},... | collective-permute-start | bytes 1179656 | tf_op jit(solution)/shard_map/ppermute | solution.py:111
  7.3 33.7 %collective-permute-start.8 = (bf16[256,768]{1,0:T(8,128)(2,1)}, bf16[256,768]{1,0:T(8,128)(2,1)S(1)}, u32[]{:S(2)}, u32[]{:S(2)}) collective-permute-start(bf16[256,768]{1,0:T(8,128)(2,1)} %pad_maximum_fusion.5), channel_id=1, source_target_pairs={{0,16},{16,0},{1,17},{17,1},{2,18},{18,2},{3,19},{19,3},{4,20},{20... | collective-permute-start | bytes 1179656 | tf_op jit(solution)/shard_map/ppermute | solution.py:108
  8.8 30.0 %collective-permute-start.4 = (bf16[256,768]{1,0:T(8,128)(2,1)}, bf16[256,768]{1,0:T(8,128)(2,1)S(1)}, u32[]{:S(2)}, u32[]{:S(2)}) collective-permute-start(bf16[256,768]{1,0:T(8,128)(2,1)} %pad_maximum_fusion.5), channel_id=1, source_target_pairs={{0,8},{2,10},{4,12},{6,14},{8,0},{10,2},{12,4},{14,6},{1,9},{3,11}... | collective-permute-start | bytes 1179656 | tf_op jit(solution)/shard_map/ppermute | solution.py:123
  11.4 9.9 %collective-permute-start.20 = (f32[512]{0:T(512)}, f32[512]{0:T(512)}, u32[]{:S(2)}, u32[]{:S(2)}) collective-permute-start(f32[512]{0:T(512)} %param.16), channel_id=1, source_target_pairs={{0,1},{1,0},{2,3},{3,2},{4,5},{5,4},{6,7},{7,6},{8,9},{9,8},{10,11... | collective-permute-start | bytes 6152 | tf_op jit(solution)/shard_map/ppermute | solution.py:138
  21.3 19.2 %copy-start.1 = (bf16[256,4096]{1,0:T(8,128)(2,1)S(1)}, bf16[256,4096]{1,0:T(8,128)(2,1)}, u32[]{:S(2)}) copy-start(bf16[256,4096]{1,0:T(8,128)(2,1)} %param.22) | copy-start | bytes 6291460
  21.3 1.5 collective-permute-start.21
  22.8 16.2 %collective-permute-start.6 = (bf16[256,768]{1,0:T(8,128)(2,1)}, bf16[256,768]{1,0:T(8,128)(2,1)S(1)}, u32[]{:S(2)}, u32[]{:S(2)}) collective-permute-start(bf16[256,768]{1,0:T(8,128)(2,1)} %pad_maximum_fusion.5), channel_id=1, source_target_pairs={{0,12},{2,14},{4,8},{6,10},{8,4},{10,6},{12,0},{14,2},{1,13},{3,15... | collective-permute-start | bytes 1179656 | tf_op jit(solution)/shard_map/ppermute | solution.py:123
  23.7 14.2 %collective-permute-start.2 = (bf16[256,1024]{1,0:T(8,128)(2,1)}, bf16[256,1024]{1,0:T(8,128)(2,1)S(1)}, u32[]{:S(2)}, u32[]{:S(2)}) collective-permute-start(bf16[256,1024]{1,0:T(8,128)(2,1)} %constant_dynamic-slice_fusion.5), channel_id=1, source_target_pairs={{0,2},{2,0},{4,6},{6,4},{8,10},{10,8},{12,14},{14,12},{1,3},{3,1},... | collective-permute-start | bytes 1572872 | tf_op jit(solution)/shard_map/ppermute | solution.py:111
  27.4 15.2 %collective-permute-start.9 = (bf16[256,768]{1,0:T(8,128)(2,1)}, bf16[256,768]{1,0:T(8,128)(2,1)S(1)}, u32[]{:S(2)}, u32[]{:S(2)}) collective-permute-start(bf16[256,768]{1,0:T(8,128)(2,1)} %collective-permute-done), channel_id=1, source_target_pairs={{0,16},{16,0},{1,17},{17,1},{2,18},{18,2},{3,19},{19,3},{4,20},{20... | collective-permute-start | bytes 1179656 | tf_op jit(solution)/shard_map/ppermute | solution.py:108
  38.0 22.6 %collective-permute-start.3 = (bf16[256,768]{1,0:T(8,128)(2,1)S(1)}, bf16[256,768]{1,0:T(8,128)(2,1)S(1)}, u32[]{:S(2)}, u32[]{:S(2)}) collective-permute-start(bf16[256,768]{1,0:T(8,128)(2,1)S(1)} %collective-permute-done.1), channel_id=1, source_target_pairs={{0,2},{2,0},{4,6},{6,4},{8,10},{10,8},{12,14},{14,12},{1,3},{3,1},... | collective-permute-start | bytes 1179656 | tf_op jit(solution)/shard_map/ppermute | solution.py:111
  38.7 28.0 %collective-permute-start.11 = (bf16[256,768]{1,0:T(8,128)(2,1)S(1)}, bf16[256,768]{1,0:T(8,128)(2,1)S(1)}, u32[]{:S(2)}, u32[]{:S(2)}) collective-permute-start(bf16[256,768]{1,0:T(8,128)(2,1)S(1)} %collective-permute-done.1), channel_id=1, source_target_pairs={{0,16},{16,0},{1,17},{17,1},{2,18},{18,2},{3,19},{19,3},{4,20},{20... | collective-permute-start | bytes 1179656 | tf_op jit(solution)/shard_map/ppermute | solution.py:108
  39.0 19.4 %collective-permute-start.7 = (bf16[256,768]{1,0:T(8,128)(2,1)S(1)}, bf16[256,768]{1,0:T(8,128)(2,1)S(1)}, u32[]{:S(2)}, u32[]{:S(2)}) collective-permute-start(bf16[256,768]{1,0:T(8,128)(2,1)S(1)} %collective-permute-done.6), channel_id=1, source_target_pairs={{0,2},{2,0},{4,6},{6,4},{8,10},{10,8},{12,14},{14,12},{1,3},{3,1},... | collective-permute-start | bytes 1179656 | tf_op jit(solution)/shard_map/ppermute | solution.py:111
  41.0 17.9 %collective-permute-start.17 = (bf16[256,768]{1,0:T(8,128)(2,1)S(1)}, bf16[256,768]{1,0:T(8,128)(2,1)S(1)}, u32[]{:S(2)}, u32[]{:S(2)}) collective-permute-start(bf16[256,768]{1,0:T(8,128)(2,1)S(1)} %collective-permute-done.6), channel_id=1, source_target_pairs={{0,16},{16,0},{1,17},{17,1},{2,18},{18,2},{3,19},{19,3},{4,20},{20... | collective-permute-start | bytes 1179656 | tf_op jit(solution)/shard_map/ppermute | solution.py:108
  42.6 22.5 %collective-permute-start.5 = (bf16[256,768]{1,0:T(8,128)(2,1)S(1)}, bf16[256,768]{1,0:T(8,128)(2,1)S(1)}, u32[]{:S(2)}, u32[]{:S(2)}) collective-permute-start(bf16[256,768]{1,0:T(8,128)(2,1)S(1)} %collective-permute-done.4), channel_id=1, source_target_pairs={{0,2},{2,0},{4,6},{6,4},{8,10},{10,8},{12,14},{14,12},{1,3},{3,1},... | collective-permute-start | bytes 1179656 | tf_op jit(solution)/shard_map/ppermute | solution.py:111
  58.4 9.9 %collective-permute-start.14 = (bf16[256,768]{1,0:T(8,128)(2,1)S(1)}, bf16[256,768]{1,0:T(8,128)(2,1)S(1)}, u32[]{:S(2)}, u32[]{:S(2)}) collective-permute-start(bf16[256,768]{1,0:T(8,128)(2,1)S(1)} %collective-permute-done.4), channel_id=1, source_target_pairs={{0,16},{16,0},{1,17},{17,1},{2,18},{18,2},{3,19},{19,3},{4,20},{20... | collective-permute-start | bytes 1179656 | tf_op jit(solution)/shard_map/ppermute | solution.py:108
  58.9 68.7 %collective-permute-start.29 = (bf16[512,1024]{1,0:T(8,128)(2,1)S(1)}, bf16[512,1024]{1,0:T(8,128)(2,1)S(1)}, u32[]{:S(2)}, u32[]{:S(2)}) collective-permute-start(bf16[512,1024]{1,0:T(8,128)(2,1)S(1)} %pad_maximum_fusion.3), channel_id=1, source_target_pairs={{0,8},{2,10},{4,12},{6,14},{8,0},{10,2},{12,4},{14,6},{1,9},{3,11}... | collective-permute-start | bytes 3145736 | tf_op jit(solution)/shard_map/ppermute | solution.py:123
  60.5 28.7 %collective-permute-start.10 = (bf16[1536,512]{1,0:T(8,128)(2,1)S(1)}, bf16[1536,512]{1,0:T(8,128)(2,1)S(1)}, u32[]{:S(2)}, u32[]{:S(2)}) collective-permute-start(bf16[1536,512]{1,0:T(8,128)(2,1)S(1)} %maximum_dynamic-update-slice_fusion.4), channel_id=1, source_target_pairs={{0,1},{1,0},{2,3},{3,2},{4,5},{5,4},{6,7},{7,6},{8,9},{9,8},{10,11... | collective-permute-start | bytes 4718600 | tf_op jit(solution)/shard_map/ppermute | solution.py:138
  65.6 12.1 %collective-permute-start.12 = (bf16[256,768]{1,0:T(8,128)(2,1)S(1)}, bf16[256,768]{1,0:T(8,128)(2,1)S(1)}, u32[]{:S(2)}, u32[]{:S(2)}) collective-permute-start(bf16[256,768]{1,0:T(8,128)(2,1)S(1)} %collective-permute-done.3), channel_id=1, source_target_pairs={{0,16},{16,0},{1,17},{17,1},{2,18},{18,2},{3,19},{19,3},{4,20},{20... | collective-permute-start | bytes 1179656 | tf_op jit(solution)/shard_map/ppermute | solution.py:108
  66.7 16.8 %collective-permute-start.18 = (bf16[256,768]{1,0:T(8,128)(2,1)S(1)}, bf16[256,768]{1,0:T(8,128)(2,1)S(1)}, u32[]{:S(2)}, u32[]{:S(2)}) collective-permute-start(bf16[256,768]{1,0:T(8,128)(2,1)S(1)} %collective-permute-done.7), channel_id=1, source_target_pairs={{0,16},{16,0},{1,17},{17,1},{2,18},{18,2},{3,19},{19,3},{4,20},{20... | collective-permute-start | bytes 1179656 | tf_op jit(solution)/shard_map/ppermute | solution.py:108
  68.3 9.6 %collective-permute-start.15 = (bf16[256,768]{1,0:T(8,128)(2,1)S(1)}, bf16[256,768]{1,0:T(8,128)(2,1)S(1)}, u32[]{:S(2)}, u32[]{:S(2)}) collective-permute-start(bf16[256,768]{1,0:T(8,128)(2,1)S(1)} %collective-permute-done.14), channel_id=1, source_target_pairs={{0,2},{2,0},{4,6},{6,4},{8,10},{10,8},{12,14},{14,12},{1,3},{3,1},... | collective-permute-start | bytes 1179656 | tf_op jit(solution)/shard_map/ppermute | solution.py:111
  77.8 7.2 %collective-permute-start.13 = (bf16[1536,512]{1,0:T(8,128)(2,1)S(1)}, bf16[1536,512]{1,0:T(8,128)(2,1)S(1)}, u32[]{:S(2)}, u32[]{:S(2)}) collective-permute-start(bf16[1536,512]{1,0:T(8,128)(2,1)S(1)} %maximum_dynamic-update-slice_fusion.6), channel_id=1, source_target_pairs={{0,1},{1,0},{2,3},{3,2},{4,5},{5,4},{6,7},{7,6},{8,9},{9,8},{10,11... | collective-permute-start | bytes 4718600 | tf_op jit(solution)/shard_map/ppermute | solution.py:138
  78.2 8.4 %collective-permute-start.16 = (bf16[1536,512]{1,0:T(8,128)(2,1)S(1)}, bf16[1536,512]{1,0:T(8,128)(2,1)S(1)}, u32[]{:S(2)}, u32[]{:S(2)}) collective-permute-start(bf16[1536,512]{1,0:T(8,128)(2,1)S(1)} %maximum_dynamic-update-slice_fusion.8), channel_id=1, source_target_pairs={{0,1},{1,0},{2,3},{3,2},{4,5},{5,4},{6,7},{7,6},{8,9},{9,8},{10,11... | collective-permute-start | bytes 4718600 | tf_op jit(solution)/shard_map/ppermute | solution.py:138
  83.7 4.4 %collective-permute-start.19 = (bf16[1536,512]{1,0:T(8,128)(2,1)S(1)}, bf16[1536,512]{1,0:T(8,128)(2,1)S(1)}, u32[]{:S(2)}, u32[]{:S(2)}) collective-permute-start(bf16[1536,512]{1,0:T(8,128)(2,1)S(1)} %maximum_dynamic-update-slice_fusion.10), channel_id=1, source_target_pairs={{0,1},{1,0},{2,3},{3,2},{4,5},{5,4},{6,7},{7,6},{8,9},{9,8},{10,11... | collective-permute-start | bytes 4718600 | tf_op jit(solution)/shard_map/ppermute | solution.py:138
  85.0 41.2 %collective-permute-start.28 = (bf16[512,1024]{1,0:T(8,128)(2,1)S(1)}, bf16[512,1024]{1,0:T(8,128)(2,1)S(1)}, u32[]{:S(2)}, u32[]{:S(2)}) collective-permute-start(bf16[512,1024]{1,0:T(8,128)(2,1)S(1)} %pad_maximum_fusion.3), channel_id=1, source_target_pairs={{0,4},{2,6},{4,0},{6,2},{8,12},{10,14},{12,8},{14,10},{1,5},{3,7},... | collective-permute-start | bytes 3145736 | tf_op jit(solution)/shard_map/ppermute | solution.py:123
  86.5 78.1 %collective-permute-start.30 = (bf16[512,1024]{1,0:T(8,128)(2,1)S(1)}, bf16[512,1024]{1,0:T(8,128)(2,1)S(1)}, u32[]{:S(2)}, u32[]{:S(2)}) collective-permute-start(bf16[512,1024]{1,0:T(8,128)(2,1)S(1)} %pad_maximum_fusion.3), channel_id=1, source_target_pairs={{4,8},{6,10},{8,4},{10,6},{5,9},{7,11},{9,5},{11,7},{20,24},{22,26... | collective-permute-start | bytes 3145736 | tf_op jit(solution)/shard_map/ppermute | solution.py:123
  88.1 14.1 %collective-permute-start.32 = (bf16[1024,256]{1,0:T(8,128)(2,1)S(1)}, bf16[1024,256]{1,0:T(8,128)(2,1)S(1)}, u32[]{:S(2)}, u32[]{:S(2)}) collective-permute-start(bf16[1024,256]{1,0:T(8,128)(2,1)S(1)} %copy-done.3), channel_id=1, source_target_pairs={{0,2},{2,0},{4,6},{6,4},{8,10},{10,8},{12,14},{14,12},{1,3},{3,1},... | collective-permute-start | bytes 1572872 | tf_op jit(solution)/shard_map/ppermute | solution.py:111
  96.1 32.3 %collective-permute-start.22 = (bf16[128,2048]{1,0:T(8,128)(2,1)S(1)}, bf16[128,2048]{1,0:T(8,128)(2,1)S(1)}, u32[]{:S(2)}, u32[]{:S(2)}) collective-permute-start(bf16[128,2048]{1,0:T(8,128)(2,1)S(1)} %get-tuple-element.96), channel_id=1, source_target_pairs={{0,16},{16,0},{1,17},{17,1},{2,18},{18,2},{3,19},{19,3},{4,20},{20... | collective-permute-start | bytes 1572872 | tf_op jit(solution)/shard_map/ppermute | solution.py:108
  103.5 26.6 %collective-permute-start.23 = (bf16[128,2048]{1,0:T(8,128)(2,1)S(1)}, bf16[128,2048]{1,0:T(8,128)(2,1)S(1)}, u32[]{:S(2)}, u32[]{:S(2)}) collective-permute-start(bf16[128,2048]{1,0:T(8,128)(2,1)S(1)} %get-tuple-element.95), channel_id=1, source_target_pairs={{0,16},{16,0},{1,17},{17,1},{2,18},{18,2},{3,19},{19,3},{4,20},{20... | collective-permute-start | bytes 1572872 | tf_op jit(solution)/shard_map/ppermute | solution.py:108
  126.3 14.9 %collective-permute-start.24 = (bf16[128,2048]{1,0:T(8,128)(2,1)S(1)}, bf16[128,2048]{1,0:T(8,128)(2,1)S(1)}, u32[]{:S(2)}, u32[]{:S(2)}) collective-permute-start(bf16[128,2048]{1,0:T(8,128)(2,1)S(1)} %get-tuple-element.96), channel_id=1, source_target_pairs={{0,2},{2,0},{4,6},{6,4},{8,10},{10,8},{12,14},{14,12},{1,3},{3,1},... | collective-permute-start | bytes 1572872 | tf_op jit(solution)/shard_map/ppermute | solution.py:111
  127.6 24.8 %collective-permute-start.25 = (bf16[128,2048]{1,0:T(8,128)(2,1)S(1)}, bf16[128,2048]{1,0:T(8,128)(2,1)S(1)}, u32[]{:S(2)}, u32[]{:S(2)}) collective-permute-start(bf16[128,2048]{1,0:T(8,128)(2,1)S(1)} %get-tuple-element.95), channel_id=1, source_target_pairs={{0,2},{2,0},{4,6},{6,4},{8,10},{10,8},{12,14},{14,12},{1,3},{3,1},... | collective-permute-start | bytes 1572872 | tf_op jit(solution)/shard_map/ppermute | solution.py:111
  128.5 36.7 %collective-permute-start.31 = (bf16[512,1024]{1,0:T(8,128)(2,1)S(1)}, bf16[512,1024]{1,0:T(8,128)(2,1)S(1)}, u32[]{:S(2)}, u32[]{:S(2)}) collective-permute-start(bf16[512,1024]{1,0:T(8,128)(2,1)S(1)} %collective-permute-done.29), channel_id=1, source_target_pairs={{4,0},{6,2},{8,12},{10,14},{5,1},{7,3},{9,13},{11,15},{20,16},{22,... | collective-permute-start | bytes 3145736 | tf_op jit(solution)/shard_map/ppermute | solution.py:123
  130.1 32.7 %collective-permute-start.26 = (bf16[128,2048]{1,0:T(8,128)(2,1)S(1)}, bf16[128,2048]{1,0:T(8,128)(2,1)S(1)}, u32[]{:S(2)}, u32[]{:S(2)}) collective-permute-start(bf16[128,2048]{1,0:T(8,128)(2,1)S(1)} %collective-permute-done.22), channel_id=1, source_target_pairs={{0,2},{2,0},{4,6},{6,4},{8,10},{10,8},{12,14},{14,12},{1,3},{3,1},... | collective-permute-start | bytes 1572872 | tf_op jit(solution)/shard_map/ppermute | solution.py:111
  141.2 29.2 %collective-permute-start.33 = (bf16[512,1024]{1,0:T(8,128)(2,1)S(1)}, bf16[512,1024]{1,0:T(8,128)(2,1)S(1)}, u32[]{:S(2)}, u32[]{:S(2)}) collective-permute-start(bf16[512,1024]{1,0:T(8,128)(2,1)S(1)} %pad_maximum_fusion.3), channel_id=1, source_target_pairs={{0,1},{1,0},{2,3},{3,2},{4,5},{5,4},{6,7},{7,6},{8,9},{9,8},{10,11... | collective-permute-start | bytes 3145736 | tf_op jit(solution)/shard_map/ppermute | solution.py:138
  152.4 12.2 %collective-permute-start.27 = (bf16[128,2048]{1,0:T(8,128)(2,1)S(1)}, bf16[128,2048]{1,0:T(8,128)(2,1)S(1)}, u32[]{:S(2)}, u32[]{:S(2)}) collective-permute-start(bf16[128,2048]{1,0:T(8,128)(2,1)S(1)} %collective-permute-done.25), channel_id=1, source_target_pairs={{0,16},{16,0},{1,17},{17,1},{2,18},{18,2},{3,19},{19,3},{4,20},{20... | collective-permute-start | bytes 1572872 | tf_op jit(solution)/shard_map/ppermute | solution.py:108
  162.7 13.0 %collective-permute-start.37 = (bf16[1024,512]{1,0:T(8,128)(2,1)S(1)}, bf16[1024,512]{1,0:T(8,128)(2,1)S(1)}, u32[]{:S(2)}, u32[]{:S(2)}) collective-permute-start(bf16[1024,512]{1,0:T(8,128)(2,1)S(1)} %pad_maximum_fusion.4), channel_id=1, source_target_pairs={{0,1},{1,0},{2,3},{3,2},{4,5},{5,4},{6,7},{7,6},{8,9},{9,8},{10,11... | collective-permute-start | bytes 3145736 | tf_op jit(solution)/shard_map/ppermute | solution.py:138
  164.6 6.5 %collective-permute-start.34 = (bf16[512,1024]{1,0:T(8,128)(2,1)S(1)}, bf16[512,1024]{1,0:T(8,128)(2,1)S(1)}, u32[]{:S(2)}, u32[]{:S(2)}) collective-permute-start(bf16[512,1024]{1,0:T(8,128)(2,1)S(1)} %collective-permute-done.28), channel_id=1, source_target_pairs={{0,1},{1,0},{2,3},{3,2},{4,5},{5,4},{6,7},{7,6},{8,9},{9,8},{10,11... | collective-permute-start | bytes 3145736 | tf_op jit(solution)/shard_map/ppermute | solution.py:138
  164.6 6.4 %collective-permute-start.35 = (bf16[512,1024]{1,0:T(8,128)(2,1)S(1)}, bf16[512,1024]{1,0:T(8,128)(2,1)S(1)}, u32[]{:S(2)}, u32[]{:S(2)}) collective-permute-start(bf16[512,1024]{1,0:T(8,128)(2,1)S(1)} %collective-permute-done.29), channel_id=1, source_target_pairs={{0,1},{1,0},{2,3},{3,2},{4,5},{5,4},{6,7},{7,6},{8,9},{9,8},{10,11... | collective-permute-start | bytes 3145736 | tf_op jit(solution)/shard_map/ppermute | solution.py:138
  165.6 5.4 %collective-permute-start.36 = (bf16[512,1024]{1,0:T(8,128)(2,1)S(1)}, bf16[512,1024]{1,0:T(8,128)(2,1)S(1)}, u32[]{:S(2)}, u32[]{:S(2)}) collective-permute-start(bf16[512,1024]{1,0:T(8,128)(2,1)S(1)} %get-tuple-element.32), channel_id=1, source_target_pairs={{0,1},{1,0},{2,3},{3,2},{4,5},{5,4},{6,7},{7,6},{8,9},{9,8},{10,11... | collective-permute-start | bytes 3145736 | tf_op jit(solution)/shard_map/ppermute | solution.py:138
  170.4 78.3 %copy-start.22 = (bf16[1024,1024]{1,0:T(8,128)(2,1)}, bf16[1024,1024]{1,0:T(8,128)(2,1)S(1)}, u32[]{:S(2)}) copy-start(bf16[1024,1024]{1,0:T(8,128)(2,1)S(1)} %multiply_convert_fusion.1) | copy-start | bytes 6291460
  170.4 48.8 %collective-permute-start.42 = (bf16[1024,512]{1,0:T(8,128)(2,1)S(1)}, bf16[1024,512]{1,0:T(8,128)(2,1)S(1)}, u32[]{:S(2)}, u32[]{:S(2)}) collective-permute-start(bf16[1024,512]{1,0:T(8,128)(2,1)S(1)} %pad_maximum_fusion.4), channel_id=1, source_target_pairs={{0,8},{2,10},{4,12},{6,14},{8,0},{10,2},{12,4},{14,6},{1,9},{3,11}... | collective-permute-start | bytes 3145736 | tf_op jit(solution)/shard_map/ppermute | solution.py:123
  175.8 71.7 %copy-start.21 = (bf16[1024,1024]{1,0:T(8,128)(2,1)}, bf16[1024,1024]{1,0:T(8,128)(2,1)S(1)}, u32[]{:S(2)}) copy-start(bf16[1024,1024]{1,0:T(8,128)(2,1)S(1)} %multiply_convert_fusion) | copy-start | bytes 6291460
  178.3 9.2 %collective-permute-start.38 = (bf16[256,512]{1,0:T(8,128)(2,1)S(1)}, bf16[256,512]{1,0:T(8,128)(2,1)S(1)}, u32[]{:S(2)}, u32[]{:S(2)}) collective-permute-start(bf16[256,512]{1,0:T(8,128)(2,1)S(1)} %get-tuple-element.92), channel_id=1, source_target_pairs={{0,16},{16,0},{1,17},{17,1},{2,18},{18,2},{3,19},{19,3},{4,20},{20... | collective-permute-start | bytes 786440 | tf_op jit(solution)/shard_map/ppermute | solution.py:108
  179.8 13.7 %collective-permute-start.39 = (bf16[256,512]{1,0:T(8,128)(2,1)S(1)}, bf16[256,512]{1,0:T(8,128)(2,1)S(1)}, u32[]{:S(2)}, u32[]{:S(2)}) collective-permute-start(bf16[256,512]{1,0:T(8,128)(2,1)S(1)} %get-tuple-element.94), channel_id=1, source_target_pairs={{0,2},{2,0},{4,6},{6,4},{8,10},{10,8},{12,14},{14,12},{1,3},{3,1},... | collective-permute-start | bytes 786440 | tf_op jit(solution)/shard_map/ppermute | solution.py:111
  180.4 13.1 %collective-permute-start.40 = (bf16[256,512]{1,0:T(8,128)(2,1)S(1)}, bf16[256,512]{1,0:T(8,128)(2,1)S(1)}, u32[]{:S(2)}, u32[]{:S(2)}) collective-permute-start(bf16[256,512]{1,0:T(8,128)(2,1)S(1)} %get-tuple-element.93), channel_id=1, source_target_pairs={{0,18},{2,16},{4,22},{6,20},{8,26},{10,24},{12,30},{14,28},{16,2},... | collective-permute-start | bytes 786440 | tf_op jit(solution)/shard_map/ppermute | solution.py:119
  219.2 2.7 collective-permute-start.43
  219.3 25.5 %collective-permute-start.48 = (bf16[1024,512]{1,0:T(8,128)(2,1)S(1)}, bf16[1024,512]{1,0:T(8,128)(2,1)S(1)}, u32[]{:S(2)}, u32[]{:S(2)}) collective-permute-start(bf16[1024,512]{1,0:T(8,128)(2,1)S(1)} %pad_maximum_fusion.4), channel_id=1, source_target_pairs={{0,4},{2,6},{4,0},{6,2},{8,12},{10,14},{12,8},{14,10},{1,5},{3,7},... | collective-permute-start | bytes 3145736 | tf_op jit(solution)/shard_map/ppermute | solution.py:123
  224.5 9.2 %collective-permute-start.44 = (bf16[256,512]{1,0:T(8,128)(2,1)S(1)}, bf16[256,512]{1,0:T(8,128)(2,1)S(1)}, u32[]{:S(2)}, u32[]{:S(2)}) collective-permute-start(bf16[256,512]{1,0:T(8,128)(2,1)S(1)} %get-tuple-element.89), channel_id=1, source_target_pairs={{0,16},{16,0},{1,17},{17,1},{2,18},{18,2},{3,19},{19,3},{4,20},{20... | collective-permute-start | bytes 786440 | tf_op jit(solution)/shard_map/ppermute | solution.py:108
  225.9 13.7 %collective-permute-start.45 = (bf16[256,512]{1,0:T(8,128)(2,1)S(1)}, bf16[256,512]{1,0:T(8,128)(2,1)S(1)}, u32[]{:S(2)}, u32[]{:S(2)}) collective-permute-start(bf16[256,512]{1,0:T(8,128)(2,1)S(1)} %get-tuple-element.91), channel_id=1, source_target_pairs={{0,2},{2,0},{4,6},{6,4},{8,10},{10,8},{12,14},{14,12},{1,3},{3,1},... | collective-permute-start | bytes 786440 | tf_op jit(solution)/shard_map/ppermute | solution.py:111
  226.6 13.1 %collective-permute-start.46 = (bf16[256,512]{1,0:T(8,128)(2,1)S(1)}, bf16[256,512]{1,0:T(8,128)(2,1)S(1)}, u32[]{:S(2)}, u32[]{:S(2)}) collective-permute-start(bf16[256,512]{1,0:T(8,128)(2,1)S(1)} %get-tuple-element.90), channel_id=1, source_target_pairs={{0,18},{2,16},{4,22},{6,20},{8,26},{10,24},{12,30},{14,28},{16,2},... | collective-permute-start | bytes 786440 | tf_op jit(solution)/shard_map/ppermute | solution.py:119
  244.8 2.7 collective-permute-start.49
  244.8 28.9 %collective-permute-start.54 = (bf16[1024,512]{1,0:T(8,128)(2,1)S(1)}, bf16[1024,512]{1,0:T(8,128)(2,1)S(1)}, u32[]{:S(2)}, u32[]{:S(2)}) collective-permute-start(bf16[1024,512]{1,0:T(8,128)(2,1)S(1)} %pad_maximum_fusion.4), channel_id=1, source_target_pairs={{4,8},{6,10},{8,4},{10,6},{5,9},{7,11},{9,5},{11,7},{20,24},{22,26... | collective-permute-start | bytes 3145736 | tf_op jit(solution)/shard_map/ppermute | solution.py:123
  245.5 27.5 %collective-permute-start.55 = (bf16[1024,512]{1,0:T(8,128)(2,1)S(1)}, bf16[1024,512]{1,0:T(8,128)(2,1)S(1)}, u32[]{:S(2)}, u32[]{:S(2)}) collective-permute-start(bf16[1024,512]{1,0:T(8,128)(2,1)S(1)} %collective-permute-done.42), channel_id=1, source_target_pairs={{4,0},{6,2},{8,12},{10,14},{5,1},{7,3},{9,13},{11,15},{20,16},{22,... | collective-permute-start | bytes 3145736 | tf_op jit(solution)/shard_map/ppermute | solution.py:123
  250.9 22.1 %collective-permute-start.50 = (bf16[256,512]{1,0:T(8,128)(2,1)S(1)}, bf16[256,512]{1,0:T(8,128)(2,1)S(1)}, u32[]{:S(2)}, u32[]{:S(2)}) collective-permute-start(bf16[256,512]{1,0:T(8,128)(2,1)S(1)} %get-tuple-element.86), channel_id=1, source_target_pairs={{0,16},{16,0},{1,17},{17,1},{2,18},{18,2},{3,19},{19,3},{4,20},{20... | collective-permute-start | bytes 786440 | tf_op jit(solution)/shard_map/ppermute | solution.py:108
  273.8 3.5 %collective-permute-start.56 = (bf16[1024,512]{1,0:T(8,128)(2,1)S(1)}, bf16[1024,512]{1,0:T(8,128)(2,1)}, u32[]{:S(2)}, u32[]{:S(2)}) collective-permute-start(bf16[1024,512]{1,0:T(8,128)(2,1)S(1)} %broadcast_select_fusion), channel_id=1, source_target_pairs={{0,1},{1,0},{2,3},{3,2},{4,5},{5,4},{6,7},{7,6},{8,9},{9,8},{10,11... | collective-permute-start | bytes 3145736 | tf_op jit(solution)/shard_map/ppermute | solution.py:138
  273.9 9.9 %collective-permute-start.41 = (bf16[256,512]{1,0:T(8,128)(2,1)}, bf16[256,512]{1,0:T(8,128)(2,1)S(1)}, u32[]{:S(2)}, u32[]{:S(2)}) collective-permute-start(bf16[256,512]{1,0:T(8,128)(2,1)} %add_convert_fusion.8), channel_id=1, source_target_pairs={{0,1},{1,0},{2,3},{3,2},{4,5},{5,4},{6,7},{7,6},{8,9},{9,8},{10,11... | collective-permute-start | bytes 786440 | tf_op jit(solution)/shard_map/ppermute | solution.py:138
  274.4 15.0 %collective-permute-start.51 = (bf16[256,512]{1,0:T(8,128)(2,1)}, bf16[256,512]{1,0:T(8,128)(2,1)S(1)}, u32[]{:S(2)}, u32[]{:S(2)}) collective-permute-start(bf16[256,512]{1,0:T(8,128)(2,1)} %get-tuple-element.88), channel_id=1, source_target_pairs={{0,2},{2,0},{4,6},{6,4},{8,10},{10,8},{12,14},{14,12},{1,3},{3,1},... | collective-permute-start | bytes 786440 | tf_op jit(solution)/shard_map/ppermute | solution.py:111
  275.8 13.6 %collective-permute-start.52 = (bf16[256,512]{1,0:T(8,128)(2,1)}, bf16[256,512]{1,0:T(8,128)(2,1)S(1)}, u32[]{:S(2)}, u32[]{:S(2)}) collective-permute-start(bf16[256,512]{1,0:T(8,128)(2,1)} %get-tuple-element.87), channel_id=1, source_target_pairs={{0,18},{2,16},{4,22},{6,20},{8,26},{10,24},{12,30},{14,28},{16,2},... | collective-permute-start | bytes 786440 | tf_op jit(solution)/shard_map/ppermute | solution.py:119
  281.7 9.2 %collective-permute-start.57 = (bf16[256,512]{1,0:T(8,128)(2,1)S(1)}, bf16[256,512]{1,0:T(8,128)(2,1)S(1)}, u32[]{:S(2)}, u32[]{:S(2)}) collective-permute-start(bf16[256,512]{1,0:T(8,128)(2,1)S(1)} %get-tuple-element.83), channel_id=1, source_target_pairs={{0,16},{16,0},{1,17},{17,1},{2,18},{18,2},{3,19},{19,3},{4,20},{20... | collective-permute-start | bytes 786440 | tf_op jit(solution)/shard_map/ppermute | solution.py:108
  282.6 17.1 %collective-permute-start.58 = (bf16[256,512]{1,0:T(8,128)(2,1)S(1)}, bf16[256,512]{1,0:T(8,128)(2,1)S(1)}, u32[]{:S(2)}, u32[]{:S(2)}) collective-permute-start(bf16[256,512]{1,0:T(8,128)(2,1)S(1)} %get-tuple-element.85), channel_id=1, source_target_pairs={{0,2},{2,0},{4,6},{6,4},{8,10},{10,8},{12,14},{14,12},{1,3},{3,1},... | collective-permute-start | bytes 786440 | tf_op jit(solution)/shard_map/ppermute | solution.py:111
  283.8 16.0 %collective-permute-start.59 = (bf16[256,512]{1,0:T(8,128)(2,1)S(1)}, bf16[256,512]{1,0:T(8,128)(2,1)S(1)}, u32[]{:S(2)}, u32[]{:S(2)}) collective-permute-start(bf16[256,512]{1,0:T(8,128)(2,1)S(1)} %get-tuple-element.84), channel_id=1, source_target_pairs={{0,18},{2,16},{4,22},{6,20},{8,26},{10,24},{12,30},{14,28},{16,2},... | collective-permute-start | bytes 786440 | tf_op jit(solution)/shard_map/ppermute | solution.py:119
  289.4 10.8 %collective-permute-start.47 = (bf16[256,512]{1,0:T(8,128)(2,1)S(1)}, bf16[256,512]{1,0:T(8,128)(2,1)S(1)}, u32[]{:S(2)}, u32[]{:S(2)}) collective-permute-start(bf16[256,512]{1,0:T(8,128)(2,1)S(1)} %add_convert_fusion.7), channel_id=1, source_target_pairs={{0,1},{1,0},{2,3},{3,2},{4,5},{5,4},{6,7},{7,6},{8,9},{9,8},{10,11... | collective-permute-start | bytes 786440 | tf_op jit(solution)/shard_map/ppermute | solution.py:138
  300.2 1.6 collective-permute-start.53
  300.4 1.8 collective-permute-start.60
  (21 other events, 78.5 us)
